TPU v7x, 128 devices: a whole 4x4x4 slice. The times are simulated.
128 devices in a mesh: sp: 16 (over z, x), tp: 8 (over y, core).
Axes of the slice: x: 4, y: 4, z: 4, core: 2. Of those that a mesh axis runs over, the one named last changes fastest.
Arguments:
- latent: bfloat16 [2, 8192, 2048], P(None, ('sp', 'tp')), may hold values from -6 to 6
- context: bfloat16 [2, 1024, 2048], P(None, 'sp'), may hold values from -6 to 6
- cond: bfloat16 [2, 2048], replicated, may hold values from -6 to 6
- ctx_cond: bfloat16 [2048], replicated, may hold values from -6 to 6
- w_shift: bfloat16 [2048, 2048], P('sp', 'tp'), may hold values from -0.125 to 0.125
- w_scale: bfloat16 [2048, 2048], P('sp', 'tp'), may hold values from -0.125 to 0.125
- w_gate: bfloat16 [2048, 2048], P('sp', 'tp'), may hold values from -0.125 to 0.125
- norm_gain: float32 [2048], replicated, may hold values from 0.1 to 1.9
- w_query: bfloat16 [2048, 2048], P(None, 'tp'), may hold values from -1.08275726 to 1.08275726
- w_key: bfloat16 [2048, 2048], P(None, 'tp'), may hold values from -0.090598056 to 0.090598056
- w_value: bfloat16 [2048, 2048], P(None, 'tp'), may hold values from -0.125 to 0.125
- w_out: bfloat16 [2048, 2048], P('tp'), may hold values from -1.5 to 1.5
- rel_bias: float32 [32, 15, 31], P('tp'), may hold values from -4 to 4
- ctx_bias: float32 [32], P('tp'), may hold values from -3.5 to -2
Outputs:
- mixed: bfloat16 [2, 8192, 2048], P(None, ('sp', 'tp'))
All inputs are finite; a program needn't handle non-finite values.
Results may differ from a plain program's by a relative error of at most 0.0154.
Values may be sent and summed in bfloat16 or wider, within the bound.
No kernel may reach another device: no remote copies, remote signals or barrier semaphores. Data moves between devices by JAX's collectives and lax.ppermute only.
A program may use at most 128 MiB of HBM per device.

v0:
```python
import jax
import jax.numpy as jnp
from jax import lax
from jax.experimental import pallas as pl
from jax.experimental.pallas import tpu as pltpu
from jax.sharding import PartitionSpec as P


HEAD_DIM = 64
GRID_W = 64
WIN_ROWS = 8
WIN_COLS = 16
EPSILON = 1e-06
MASKED = -1e30
REACH = WIN_ROWS // 2
BIAS_BLOCKS = 7
RESIDENT = pl.BlockSpec(memory_space=pltpu.VMEM)


def copy_for_each(shard, axis):
    length = lax.axis_size(axis)
    return lax.all_to_all(
        jnp.broadcast_to(shard[None], (length, *shard.shape)), axis, 0, 0, tiled=True
    )


def silu_rows(values):
    return jax.nn.silu(values.astype(jnp.float32)).astype(jnp.bfloat16)


def modulation_parts(place, cond, ctx_cond, weights, copies):
    samples = cond.shape[0]
    rows, cols = weights[0].shape

    def body(place_ref, cond_ref, ctx_ref, shift_ref, scale_ref, gate_ref, out_ref, wide):
        at = pl.multiple_of(place_ref[0] * rows, rows)
        ada = silu_rows(cond_ref[:, pl.ds(at, rows)])
        wide[...] = ctx_ref[...].astype(jnp.float32).reshape(1, ctx_ref.shape[0])
        ada_ctx = silu_rows(wide[:, pl.ds(at, rows)])
        both = jnp.concatenate([ada.astype(jnp.float32), ada_ctx.astype(jnp.float32)], axis=0)
        both = both.astype(jnp.bfloat16)
        result = jnp.concatenate(
            [
                jnp.dot(both, shift_ref[...], preferred_element_type=jnp.float32),
                jnp.dot(both, scale_ref[...], preferred_element_type=jnp.float32),
                jnp.dot(ada, gate_ref[...], preferred_element_type=jnp.float32),
            ],
            axis=0,
        )
        for copy in range(copies):
            out_ref[copy] = result

    return pl.pallas_call(
        body,
        in_specs=[pl.BlockSpec(memory_space=pltpu.SMEM)]
        + [pl.BlockSpec(memory_space=pltpu.VMEM)] * 5,
        out_shape=jax.ShapeDtypeStruct((copies, 3 * samples + 2, cols), jnp.float32),
        scratch_shapes=[pltpu.VMEM((1, ctx_cond.shape[0]), jnp.float32)],
        name="modulation_parts",
    )(place, cond, ctx_cond, *weights)


def resident(array):
    return pltpu.with_memory_space_constraint(array, pltpu.VMEM)


def whole(shape):
    return pl.BlockSpec(shape, lambda *_: (0,) * len(shape))


def modulation_row(tiles, row):
    return jnp.concatenate([tiles[tile, row : row + 1, :] for tile in range(tiles.shape[0])], axis=1)


def project(rows, gain, modulation, weights, row_of, block, ends, sample=None, buffers=()):
    samples, count, width = rows.shape
    every = modulation.shape[1] // 3 + 1
    chosen = range(samples) if sample is None else (sample,)
    begin = chosen[0]
    cols = weights[0].shape[1]
    first, last = ends if ends else (0, 0)
    steps = count // block

    def body(rows_ref, gain_ref, tiles_ref, *refs):
        weight_refs, out_refs = refs[: len(weights)], refs[len(weights) + len(buffers) : -2]
        factor_ref, shift_ref = refs[-2:]
        turn, step = pl.program_id(0), pl.program_id(1)

        for number in chosen:

            @pl.when((turn == number - begin) & (step == 0))
            def _(number=number):
                row = row_of + number
                factor_ref[...] = gain_ref[...] * (1.0 + modulation_row(tiles_ref, every + row))
                shift_ref[...] = modulation_row(tiles_ref, row)

        floats = rows_ref[0].astype(jnp.float32)
        inverse = lax.rsqrt(jnp.mean(floats * floats, axis=-1, keepdims=True) + EPSILON)
        hidden = (floats * inverse * factor_ref[...] + shift_ref[...]).astype(jnp.bfloat16)
        pair = [
            jnp.dot(hidden, ref[...], preferred_element_type=jnp.float32).astype(jnp.bfloat16)
            for ref in weight_refs[:2]
        ]
        if not ends:
            out_refs[0][0, :, :cols] = pair[0]
            out_refs[0][0, :, cols:] = pair[1]
            return
        out_refs[0][0, :, :cols] = pair[0]
        out_refs[0][0, :, cols:] = pair[1]
        query = jnp.dot(hidden, weight_refs[2][...], preferred_element_type=jnp.float32)
        query = query.astype(jnp.bfloat16).astype(jnp.float32) * HEAD_DIM**-0.5
        out_refs[1][0] = query.astype(jnp.bfloat16)
        for number in range(steps):
            low = number * block
            for out_ref, start, stop in (
                (out_refs[2], 0, first),
                (out_refs[3], count - last, count),
            ):
                lo, hi = max(low, start), min(low + block, stop)
                if lo < hi:

                    @pl.when(step == number)
                    def _(out_ref=out_ref, start=start, lo=lo, hi=hi, low=low):
                        for index in range(2):
                            out_ref[
                                0, lo - start : hi - start, index * cols : (index + 1) * cols
                            ] = pair[index][lo - low : hi - low]

    def blocks(size):
        return pl.BlockSpec((1, block, size), lambda s, i: (begin + s, i, 0))

    if ends:
        out_specs = [blocks(2 * cols), blocks(cols)]
        out_shape = [(samples, count, 2 * cols), (samples, count, cols)]
        for length in ends:
            out_specs += [pl.BlockSpec((1, length, 2 * cols), lambda s, i: (begin + s, 0, 0))]
            out_shape += [(samples, length, 2 * cols)]
    else:
        out_specs = [blocks(2 * cols)]
        out_shape = [(samples, count, 2 * cols)]
    return pl.pallas_call(
        body,
        grid=(len(chosen), steps),
        in_specs=[blocks(width), whole((1, width)), RESIDENT]
        + [RESIDENT] * len(weights)
        + [pl.BlockSpec(memory_space=pl.ANY)] * len(buffers),
        out_specs=out_specs,
        out_shape=[jax.ShapeDtypeStruct(shape, jnp.bfloat16) for shape in out_shape],
        scratch_shapes=[pltpu.VMEM((1, width), jnp.float32)] * 2,
        input_output_aliases={3 + len(weights) + i: i for i in range(len(buffers))},
        compiler_params=pltpu.CompilerParams(vmem_limit_bytes=24 * 2**20),
        name="project",
    )(rows, gain, modulation, *weights, *buffers)


def bias_table(rel_bias):
    heads, offsets, spread = rel_bias.shape
    slots = 2 * BIAS_BLOCKS + 2
    padded = jnp.pad(rel_bias, ((0, 0), (0, slots - offsets), (0, 128 - spread)))
    padded = padded.reshape(heads * slots, 128)

    def body(rel_ref, out_ref):
        query = lax.broadcasted_iota(jnp.int32, (GRID_W, 128), 0)
        lane = lax.broadcasted_iota(jnp.int32, (GRID_W, 128), 1)
        low = lane < GRID_W
        key = jnp.where(low, lane, lane - GRID_W)
        start = jnp.clip(query - WIN_COLS // 2, 0, GRID_W - WIN_COLS)
        inside = (key >= start) & (key < start + WIN_COLS)

        def diagonal(head, slot, move):
            row = jnp.broadcast_to(rel_ref[pl.ds(head * slots + slot, 1), :], (GRID_W, 128))
            return pltpu.roll(row, (128 - (WIN_COLS - 1) + move) % 128, 1, stride=1, stride_axis=0)

        for parity in range(2):
            for head in range(heads):
                for block in range(BIAS_BLOCKS):
                    slot = 2 * block + parity
                    both = jnp.where(
                        low, diagonal(head, slot, 0), diagonal(head, slot + 1, GRID_W)
                    )
                    out_ref[
                        parity, head * GRID_W : (head + 1) * GRID_W, block * 128 : (block + 1) * 128
                    ] = jnp.where(inside, both, MASKED)

    return pl.pallas_call(
        body,
        out_shape=jax.ShapeDtypeStruct((2, heads * GRID_W, BIAS_BLOCKS * 128), jnp.float32),
        compiler_params=pltpu.CompilerParams(vmem_limit_bytes=16 * 2**20),
        name="bias_table",
    )(padded)


def head_masks(cols):
    lane = lax.broadcasted_iota(jnp.int32, (GRID_W, cols), 1)
    return [(lane >= low) & (lane < low + HEAD_DIM) for low in range(0, cols, HEAD_DIM)]


def spread_heads(query, masks):
    return jnp.concatenate(
        [jnp.where(mask, query, jnp.zeros_like(query)) for mask in masks], axis=0
    )


def gather_heads(values, masks):
    result = jnp.where(masks[0], values[:GRID_W], 0.0)
    for h in range(1, len(masks)):
        result = jnp.where(masks[h], values[h * GRID_W : (h + 1) * GRID_W], result)
    return result


def weighed(scores, values, masks):
    top = jnp.max(scores, axis=-1, keepdims=True)
    exps = jnp.exp(scores - top)
    total = jnp.sum(exps, axis=-1, keepdims=True)
    mixed = jnp.dot(exps.astype(jnp.bfloat16), values, preferred_element_type=jnp.float32)
    return [gather_heads(array, masks) for array in (mixed, top, total)]


def attend_near(place, query, before, pair, after, table, rows_all, per):
    samples, tokens, cols = query.shape
    rows_dev = tokens // GRID_W
    near_keys = WIN_ROWS * GRID_W
    ahead, behind = before.shape[1], after.shape[1]
    padded = ahead + tokens + behind
    lanes = -(-padded // 128) * 128
    bf16, f32 = jnp.bfloat16, jnp.float32

    def body(place_ref, q_ref, before_ref, pair_ref, after_ref, table_ref, *refs):
        out_refs, (near_t, values) = refs[:3], refs[3:]
        sample, step = pl.program_id(0), pl.program_id(1)

        @pl.when(step == 0)
        def _():
            values[0:ahead] = before_ref[sample, :, cols:]
            values[ahead : ahead + tokens] = pair_ref[0, :, cols:]
            values[ahead + tokens : padded] = after_ref[sample, :, cols:]
            fill = jnp.zeros((lanes - padded, cols), bf16)
            near_t[0, :, :ahead] = before_ref[sample, :, :cols].T
            near_t[0, :, ahead : ahead + tokens] = pair_ref[0, :, :cols].T
            near_t[0, :, ahead + tokens :] = jnp.concatenate(
                [after_ref[sample, :, :cols], fill], axis=0
            ).T
            near_t[1] = jnp.concatenate(
                [
                    before_ref[sample, GRID_W:, :cols],
                    pair_ref[0, :, :cols],
                    after_ref[sample, :, :cols],
                    fill,
                    jnp.zeros((GRID_W, cols), bf16),
                ],
                axis=0,
            ).T

        base = place_ref[0] * rows_dev
        masks = head_masks(cols)
        scores, starts = [], []
        for r in range(per):
            actual = base + step * per + r
            start = jnp.clip(actual - REACH, 0, rows_all - WIN_ROWS)
            local = start - base + REACH
            offset = start - actual + WIN_ROWS - 1
            spread = spread_heads(q_ref[0, r * GRID_W : (r + 1) * GRID_W], masks)
            column = pl.multiple_of((local // 2) * 128, 128)
            keys_t = near_t[local % 2, :, pl.ds(column, near_keys)]
            bias_at = pl.multiple_of((offset // 2) * 128, 128)
            scores.append(
                jnp.dot(spread, keys_t, preferred_element_type=f32)
                + table_ref[offset % 2, :, pl.ds(bias_at, near_keys)]
            )
            starts.append(pl.multiple_of(local * GRID_W, GRID_W))
        for r in range(per):
            parts = weighed(scores[r], values[pl.ds(starts[r], near_keys), :], masks)
            for out_ref, part in zip(out_refs, parts):
                out_ref[0, r * GRID_W : (r + 1) * GRID_W] = part

    def of_sample(array):
        return pl.BlockSpec((1, *array.shape[1:]), lambda s, i: (s, 0, 0))

    rows_spec = pl.BlockSpec((1, per * GRID_W, cols), lambda s, i: (s, i, 0))
    return pl.pallas_call(
        body,
        grid=(samples, rows_dev // per),
        in_specs=[
            pl.BlockSpec(memory_space=pltpu.SMEM),
            rows_spec,
            RESIDENT,
            of_sample(pair),
            RESIDENT,
            RESIDENT,
        ],
        out_specs=[rows_spec] * 3,
        out_shape=[jax.ShapeDtypeStruct((samples, tokens, cols), f32)] * 3,
        scratch_shapes=[
            pltpu.VMEM((2, cols, lanes), bf16),
            pltpu.VMEM((padded, cols), bf16),
        ],
        compiler_params=pltpu.CompilerParams(vmem_limit_bytes=32 * 2**20),
        name="attend_near",
    )(place, query, before, pair, after, table)


def attend_far(query, ctx_pairs, ctx_bias, near, per):
    samples, tokens, cols = query.shape
    rows_dev = tokens // GRID_W
    ctx_rows = ctx_pairs[0].shape[2]
    members = [array.shape[0] for array in ctx_pairs]
    ctx_count = sum(members) * ctx_rows
    bf16, f32 = jnp.bfloat16, jnp.float32

    def body(q_ref, *refs):
        ctx_refs = refs[: len(members)]
        cb_ref, mixed_ref, top_ref, total_ref, out_ref, far_t, values = refs[len(members) :]
        sample, step = pl.program_id(0), pl.program_id(1)

        @pl.when(step == 0)
        def _():
            at = 0
            for ctx_ref, count in zip(ctx_refs, members):
                for member in range(count):
                    low = at + member * ctx_rows
                    values[low : low + ctx_rows] = ctx_ref[member, sample, :, cols:]
                size = count * ctx_rows
                block = jnp.concatenate(
                    [ctx_ref[member, sample, :, :cols] for member in range(count)], axis=0
                )
                far_t[:, at : at + size] = block.T
                at += size

        masks = head_masks(cols)
        context_bias = jnp.concatenate(
            [jnp.full((GRID_W, cols), cb_ref[h], f32) for h in range(len(masks))], axis=0
        )
        scores = [
            jnp.dot(
                spread_heads(q_ref[0, r * GRID_W : (r + 1) * GRID_W], masks),
                far_t[...],
                preferred_element_type=f32,
            )
            for r in range(per)
        ]
        for r in range(per):
            mixed, top, total = weighed(scores[r], values[...], masks)
            at = slice(r * GRID_W, (r + 1) * GRID_W)
            top = top + gather_heads(context_bias, masks)
            near_top = top_ref[0, at]
            highest = jnp.maximum(top, near_top)
            far_part = jnp.exp(top - highest)
            near_part = jnp.exp(near_top - highest)
            total = total * far_part + total_ref[0, at] * near_part
            mixed = mixed * far_part + mixed_ref[0, at] * near_part
            out_ref[r, 0] = (mixed / total).astype(bf16)

    rows_spec = pl.BlockSpec((1, per * GRID_W, cols), lambda s, i: (s, i, 0))
    return pl.pallas_call(
        body,
        grid=(samples, rows_dev // per),
        in_specs=[
            rows_spec,
        ]
        + [RESIDENT] * len(members)
        + [pl.BlockSpec(memory_space=pltpu.SMEM)]
        + [rows_spec] * 3,
        out_specs=pl.BlockSpec((per, 1, GRID_W, cols), lambda s, i: (i, s, 0, 0)),
        out_shape=jax.ShapeDtypeStruct((rows_dev, samples, GRID_W, cols), bf16),
        scratch_shapes=[
            pltpu.VMEM((cols, ctx_count), bf16),
            pltpu.VMEM((ctx_count, cols), bf16),
        ],
        compiler_params=pltpu.CompilerParams(vmem_limit_bytes=32 * 2**20),
        name="attend_far",
    )(query, *ctx_pairs, ctx_bias, *near)


def finish(attended, w_out, latent, modulation, tiles):
    groups, _, _ = attended.shape
    samples, tokens, width = latent.shape
    block = modulation.shape[2] * tiles
    first = modulation.shape[1] - samples

    def body(att_ref, w_ref, latent_ref, tile_ref, out_ref):
        low = pl.program_id(0) * tiles
        everything = jnp.concatenate([att_ref[group] for group in range(groups)], axis=1)
        update = jnp.dot(everything, w_ref[...], preferred_element_type=jnp.float32)
        for s in range(samples):
            gate = jnp.concatenate(
                [tile_ref[low + t, first + s : first + s + 1, :] for t in range(tiles)], axis=1
            )
            part = update[s * tokens : (s + 1) * tokens]
            out_ref[s] = (latent_ref[s].astype(jnp.float32) + gate * part).astype(jnp.bfloat16)

    return pl.pallas_call(
        body,
        grid=(width // block,),
        in_specs=[
            whole(attended.shape),
            pl.BlockSpec((width, block), lambda i: (0, i)),
            pl.BlockSpec((samples, tokens, block), lambda i: (0, 0, i)),
            RESIDENT,
        ],
        out_specs=pl.BlockSpec((samples, tokens, block), lambda i: (0, 0, i)),
        out_shape=jax.ShapeDtypeStruct(latent.shape, latent.dtype),
        name="finish",
    )(attended, w_out, latent, modulation)


def shifted(size, side, stride, value):
    span = side * stride
    return [(i, i // span * span + (i + value * stride) % span) for i in range(size)]


def from_line(block, axis, side, stride):
    size = lax.axis_size(axis)
    return [block] + [
        lax.ppermute(block, axis, shifted(size, side, stride, value)) for value in range(1, side)
    ]


def computation(
    latent,
    context,
    cond,
    ctx_cond,
    w_shift,
    w_scale,
    w_gate,
    norm_gain,
    w_query,
    w_key,
    w_value,
    w_out,
    rel_bias,
    ctx_bias,
):
    samples, tokens_dev, width = latent.shape
    local_cols = w_shift.shape[1]
    sp_index = lax.axis_index("sp")
    sp_size, tp_size = lax.axis_size("sp"), lax.axis_size("tp")
    place = jnp.full((1,), sp_index, jnp.int32)
    gathered = lax.all_gather(latent, "tp", axis=1, tiled=True)
    parts = modulation_parts(place, cond, ctx_cond, (w_shift, w_scale, w_gate), sp_size)
    parts, w_out_own = lax.optimization_barrier((parts, w_out))
    w_out_all = lax.all_gather(w_out_own, "tp", axis=0, tiled=True)
    table = bias_table(rel_bias)
    summed = jnp.sum(lax.all_to_all(parts, "sp", 0, 0, tiled=True), axis=0)
    summed, table = lax.optimization_barrier((summed, table))
    modulation = resident(copy_for_each(summed, "tp"))
    w_query, w_key, w_value = resident(w_query), resident(w_key), resident(w_value)
    table = resident(table)

    gain = norm_gain[None, :]
    ctx_rows = context.shape[1]
    (ctx_pair,) = project(
        context.reshape(1, samples * ctx_rows, width),
        gain,
        modulation,
        (w_key, w_value),
        samples,
        samples * ctx_rows,
        None,
    )
    ctx_pair = ctx_pair.reshape(samples, ctx_rows, 2 * local_cols)
    ctx_pairs = from_line(ctx_pair, "sp", 4, 1)
    up = [(i, i + 1) for i in range(sp_size - 1)]
    down = [(j, i) for i, j in up]
    gathered = pltpu.with_memory_space_constraint(gathered, pltpu.HBM)
    ends = ((WIN_ROWS - REACH - 1) * GRID_W, REACH * GRID_W)
    w_triple = (w_key, w_value, w_query)
    outs = project(gathered, gain, modulation, w_triple, 0, 256, ends, 0)
    ctx_pairs, outs = lax.optimization_barrier((ctx_pairs, outs))
    ctx_line = jnp.stack(ctx_pairs)
    below = lax.ppermute(ctx_line, "sp", shifted(sp_size, 4, 4, 1))
    above = lax.ppermute(ctx_line, "sp", shifted(sp_size, 4, 4, 3))
    for s in range(1, samples):
        outs = project(gathered, gain, modulation, w_triple, 0, 256, ends, s, outs)
    pair, query, first, last = outs
    before = resident(lax.ppermute(last, "sp", up))
    after = resident(lax.ppermute(first, "sp", down))
    rows_all = pair.shape[1] // GRID_W * sp_size
    ctx_pairs = [
        ctx_line,
        below,
        above,
        lax.ppermute(below[:2], "sp", shifted(sp_size, 4, 4, 1)),
        lax.ppermute(above[2:], "sp", shifted(sp_size, 4, 4, 3)),
    ]
    ctx_pairs = [resident(array) for array in ctx_pairs]
    near = attend_near(place, query, before, pair, after, table, rows_all, 4)
    attended = attend_far(query, ctx_pairs, ctx_bias, near, 4)
    attended = attended.reshape(tp_size, samples * tokens_dev, local_cols)
    attended = lax.all_to_all(attended, "tp", 0, 0, tiled=True)
    return finish(attended, w_out_all, latent, modulation, 4)


def solution(mesh):
    return jax.shard_map(
        computation,
        mesh=mesh,
        in_specs=(
            P(None, ("sp", "tp"), None),
            P(None, "sp", None),
            P(),
            P(),
            P("sp", "tp"),
            P("sp", "tp"),
            P("sp", "tp"),
            P(),
            P(None, "tp"),
            P(None, "tp"),
            P(None, "tp"),
            P("tp", None),
            P("tp", None, None),
            P("tp"),
        ),
        out_specs=P(None, ("sp", "tp"), None),
        check_vma=False,
    )
```

profile of v0, /device:TPU:32, one launch (start us, length us, event | category | flops | bytes accessed | tf_op | source)
XLA Modules:
  0.0 117.5 jit_solution(6311627193532384985)
XLA Ops:
  6.5 0.0 all-gather.3.cloned.1.call-start
  6.6 0.7 all-gather.3.cloned.1.call-update
  7.3 0.0 all-gather.5.cloned.1.call-start
  7.3 1.9 %modulation_parts.1 = f32[16,8,256]{2,1,0:T(8,128)} custom-call(s32[1]{0:T(128)} %bitcast.1.place_ref, bf16[2,2048]{1,0:T(2,128)(2,1)} %cond_ref.1, bf16[2048]{0:T(1024)(128)(2,1)} %ctx_ref.1, bf16[128,256]{1,0:T(8,128)(2,1)} %shift_ref.1, bf16[128,256]{1,0:T(8,128)(2,1)} %scale_ref.1, bf16[128,256]{1,0:T(8,128)(2,1)} %gate_ref.1), custom_call_target="tpu_custom_call" | custom-call | tf_op jit(solution)/shard_map/modulation_parts/pallas_call | solution.py:53
  9.3 0.0 all-gather.5.cloned.1.call-update
  9.3 7.9 %all-to-all-start = ((f32[16,8,256]{2,1,0:T(8,128)}), f32[16,8,256]{2,1,0:T(8,128)S(1)}, u32[]{:S(2)}, u32[]{:S(2)}) async-start(f32[16,8,256]{2,1,0:T(8,128)} %modulation_parts.1), calls=%async_computation | async-start | bytes 262144 | tf_op jit(solution)/shard_map/all_to_all | solution.py:444
  17.2 0.8 copy.20
  18.0 1.0 bias_table.1.table_ref
  19.0 0.0 copy-start.2
  19.0 1.2 %copy-done.2 = f32[2,256,896]{2,1,0:T(8,128)} copy-done((f32[2,256,896]{2,1,0:T(8,128)}, f32[2,256,896]{2,1,0:T(8,128)S(1)}, u32[]{:S(2)}) %copy-start.2) | copy-done | bytes 1835032
  20.2 3.3 %all-to-all-done = f32[16,8,256]{2,1,0:T(8,128)S(1)} async-done(((f32[16,8,256]{2,1,0:T(8,128)}), f32[16,8,256]{2,1,0:T(8,128)S(1)}, u32[]{:S(2)}, u32[]{:S(2)}) %all-to-all-start) | async-done | bytes 131104 | tf_op jit(solution)/shard_map/all_to_all | solution.py:444
  23.5 10.8 %all_to_all.15.tiles_ref.tile_ref = f32[8,8,256]{2,1,0:T(8,128)S(1)} all-to-all(f32[8,8,256]{2,1,0:T(8,128)S(1)} %broadcast_in_dim.14), channel_id=1, replica_groups=mesh['sp'=16,'tp'=8] {'tp'}, dimensions={0} | all-to-all | bytes 131072 | tf_op jit(solution)/shard_map/all_to_all | solution.py:22
  34.3 0.0 copy-done.6
  34.3 0.0 copy-done
  34.3 0.0 copy-done.1
  34.3 0.0 copy-start.5
  34.4 1.1 copy-done.5
  35.4 0.6 project.3
  36.1 0.6 collective-permute-start
  36.7 2.2 %collective-permute-start.1 = (bf16[2,64,512]{2,1,0:T(8,128)(2,1)S(1)}, bf16[2,64,512]{2,1,0:T(8,128)(2,1)}, u32[]{:S(2)}, u32[]{:S(2)}) collective-permute-start(bf16[2,64,512]{2,1,0:T(8,128)(2,1)S(1)} %bitcast.13), channel_id=1, source_target_pairs={{0,16},{8,24},{16,0},{24,8},{32,48},{40,56},{48,32},{56,40},{64,80... | collective-permute-start | bytes 393224 | tf_op jit(solution)/shard_map/ppermute | solution.py:414
  38.8 1.4 %collective-permute-start.2 = (bf16[2,64,512]{2,1,0:T(8,128)(2,1)S(1)}, bf16[2,64,512]{2,1,0:T(8,128)(2,1)}, u32[]{:S(2)}, u32[]{:S(2)}) collective-permute-start(bf16[2,64,512]{2,1,0:T(8,128)(2,1)S(1)} %bitcast.14), channel_id=1, source_target_pairs={{0,24},{8,0},{16,8},{24,16},{32,56},{40,32},{48,40},{56,48},{64,88... | collective-permute-start | bytes 393224 | tf_op jit(solution)/shard_map/ppermute | solution.py:414
  40.2 3.6 %all-gather.3.cloned.1.call-done.rows_ref = bf16[2,512,2048]{2,1,0:T(8,128)(2,1)} async-done(((bf16[2,64,2048]{2,1,0:T(8,128)(2,1)}), bf16[2,512,2048]{2,1,0:T(8,128)(2,1)}) %all-gather.3.cloned.1.call-update) | async-done | bytes 4194320 | tf_op jit(solution)/shard_map/all_gather | solution.py:439
  43.9 0.0 copy-done.4
  43.9 3.9 %project.4 = (bf16[2,512,512]{2,1,0:T(8,128)(2,1)S(1)}, bf16[2,512,256]{2,1,0:T(8,128)(2,1)S(1)}, bf16[2,192,512]{2,1,0:T(8,128)(2,1)S(1)}, bf16[2,256,512]{2,1,0:T(8,128)(2,1)S(1)}) custom-call(bf16[2,512,2048]{2,1,0:T(8,128)(2,1)} %all-gather.3.cloned.1.call-done.rows_ref, f32[1,2048]{1,0:T(1,128)S(1)} %bitcast.18, ...), custom_call_target="tpu_custom_call" | custom-call | tf_op jit(solution)/shard_map/project/pallas_call | solution.py:141
  47.8 0.0 collective-permute-done
  47.8 0.0 collective-permute-done.1
  47.8 0.0 collective-permute-done.2
  47.8 1.0 pad_maximum_fusion.refs_0_
  48.9 0.0 copy-start.3
  48.9 1.6 %collective-permute-start.3 = (bf16[4,2,64,512]{3,2,1,0:T(8,128)(2,1)S(1)}, bf16[4,2,64,512]{3,2,1,0:T(8,128)(2,1)S(1)}, u32[]{:S(2)}, u32[]{:S(2)}) collective-permute-start(bf16[4,2,64,512]{3,2,1,0:T(8,128)(2,1)S(1)} %pad_maximum_fusion.refs_0_), channel_id=1, source_target_pairs={{0,32},{8,40},{16,48},{24,56},{32,64},{40,72},{48,80},{56,88},{64,... | collective-permute-start | bytes 1572872 | tf_op jit(solution)/shard_map/ppermute | solution.py:471
  50.5 0.5 collective-permute-start.4
  51.0 3.9 %project.5 = (bf16[2,512,512]{2,1,0:T(8,128)(2,1)S(1)}, bf16[2,512,256]{2,1,0:T(8,128)(2,1)S(1)}, bf16[2,192,512]{2,1,0:T(8,128)(2,1)S(1)}, bf16[2,256,512]{2,1,0:T(8,128)(2,1)S(1)}) custom-call(bf16[2,512,2048]{2,1,0:T(8,128)(2,1)} %all-gather.3.cloned.1.call-done.rows_ref, ...), custom_call_target="tpu_custom_call", output_to_operand_aliasing={{0}: (6, {}), {1}: (7, {}), {2}: (8, {}), {3}: (9, {})} | custom-call | tf_op jit(solution)/shard_map/project/pallas_call | solution.py:141
  54.9 0.0 copy-start.7
  54.9 3.4 %collective-permute-start.7 = (bf16[2,256,512]{2,1,0:T(8,128)(2,1)S(1)}, bf16[2,256,512]{2,1,0:T(8,128)(2,1)S(1)}, u32[]{:S(2)}, u32[]{:S(2)}) collective-permute-start(bf16[2,256,512]{2,1,0:T(8,128)(2,1)S(1)} %get-tuple-element.43), channel_id=1, source_target_pairs={{0,8},{8,16},{16,24},{24,32},{32,40},{40,48},{48,56},{56,64},{64,7... | collective-permute-start | bytes 1572872 | tf_op jit(solution)/shard_map/ppermute | solution.py:476
  58.3 4.7 %collective-permute-start.8 = (bf16[2,192,512]{2,1,0:T(8,128)(2,1)S(1)}, bf16[2,192,512]{2,1,0:T(8,128)(2,1)S(1)}, u32[]{:S(2)}, u32[]{:S(2)}) collective-permute-start(bf16[2,192,512]{2,1,0:T(8,128)(2,1)S(1)} %get-tuple-element.45), channel_id=1, source_target_pairs={{8,0},{16,8},{24,16},{32,24},{40,32},{48,40},{56,48},{64,56},{72,6... | collective-permute-start | bytes 1179656 | tf_op jit(solution)/shard_map/ppermute | solution.py:477
  63.0 11.2 %collective-permute-done.3.refs_1_ = bf16[4,2,64,512]{3,2,1,0:T(8,128)(2,1)S(1)} collective-permute-done((bf16[4,2,64,512]{3,2,1,0:T(8,128)(2,1)S(1)}, bf16[4,2,64,512]{3,2,1,0:T(8,128)(2,1)S(1)}, u32[]{:S(2)}, u32[]{:S(2)}) %collective-permute-start.3) | collective-permute-done | bytes 524320 | tf_op jit(solution)/shard_map/ppermute | solution.py:471
  74.3 1.6 %collective-permute-start.5 = (bf16[2,2,64,512]{3,2,1,0:T(8,128)(2,1)S(1)}, bf16[2,2,64,512]{3,2,1,0:T(8,128)(2,1)S(1)}, u32[]{:S(2)}, u32[]{:S(2)}) collective-permute-start(bf16[2,2,64,512]{3,2,1,0:T(8,128)(2,1)S(1)} %slice.8), channel_id=1, source_target_pairs={{0,32},{8,40},{16,48},{24,56},{32,64},{40,72},{48,80},{56,88},{64,... | collective-permute-start | bytes 786440 | tf_op jit(solution)/shard_map/ppermute | solution.py:483
  75.9 0.0 collective-permute-done.4.refs_2_
  75.9 0.5 collective-permute-start.6
  76.5 0.0 collective-permute-done.8.after_ref
  76.5 0.0 collective-permute-done.7.before_ref
  76.5 0.0 copy-done.3
  76.5 5.2 %attend_near.1 = (f32[2,512,256]{2,1,0:T(8,128)S(1)}, f32[2,512,256]{2,1,0:T(8,128)S(1)}, f32[2,512,256]{2,1,0:T(8,128)S(1)}) custom-call(s32[1]{0:T(128)} %bitcast.1.place_ref, bf16[2,512,256]{2,1,0:T(8,128)(2,1)S(1)} %get-tuple-element.38.q_ref, bf16[2,256,512]{2,1,0:T(8,128)(2,1)S(1)} %collective-permute-done.7.before_ref, ...), custom_call_target="tpu_custom_call" | custom-call | tf_op jit(solution)/shard_map/attend_near/pallas_call | solution.py:280
  81.7 0.3 collective-permute-done.5.refs_3_
  82.0 1.4 %collective-permute-done.6.refs_4_ = bf16[2,2,64,512]{3,2,1,0:T(8,128)(2,1)S(1)} collective-permute-done((bf16[2,2,64,512]{3,2,1,0:T(8,128)(2,1)S(1)}, bf16[2,2,64,512]{3,2,1,0:T(8,128)(2,1)S(1)}, u32[]{:S(2)}, u32[]{:S(2)}) %collective-permute-start.6) | collective-permute-done | bytes 262176 | tf_op jit(solution)/shard_map/ppermute | solution.py:484
  83.4 8.0 %attend_far.1 = bf16[8,2,64,256]{3,2,1,0:T(8,128)(2,1)S(1)} custom-call(bf16[2,512,256]{2,1,0:T(8,128)(2,1)S(1)} %get-tuple-element.38.q_ref, bf16[4,2,64,512]{3,2,1,0:T(8,128)(2,1)S(1)} %pad_maximum_fusion.refs_0_, bf16[4,2,64,512]{3,2,1,0:T(8,128)(2,1)S(1)} %collective-permute-done.3.refs_1_, bf16[4,2,64,512]{3,2,1,0:T(8,128)(2,1)S(1)} %collective-permute-done.4.refs_2_, ...), custom_call_target="tpu_custom_call" | custom-call | tf_op jit(solution)/shard_map/attend_far/pallas_call | solution.py:354
  91.4 13.4 %all_to_all.16.att_ref = bf16[8,128,256]{2,1,0:T(8,128)(2,1)} all-to-all(bf16[8,128,256]{2,1,0:T(8,128)(2,1)S(1)} %bitcast.10), channel_id=1, replica_groups=mesh['sp'=16,'tp'=8] {'tp'}, dimensions={0} | all-to-all | bytes 1048576 | tf_op jit(solution)/shard_map/all_to_all | solution.py:490
  104.9 5.8 %finish.1 = bf16[2,64,2048]{2,1,0:T(8,128)(2,1)} custom-call(bf16[8,128,256]{2,1,0:T(8,128)(2,1)} %all_to_all.16.att_ref, bf16[2048,2048]{1,0:T(8,128)(2,1)} %all-gather.5.cloned.1.call-done.w_ref, bf16[2,64,2048]{2,1,0:T(8,128)(2,1)} %latent_ref.1, f32[8,8,256]{2,1,0:T(8,128)S(1)} %all_to_all.15.tiles_ref.tile_ref), custom_call_target="tpu_custom_call" | custom-call | tf_op jit(solution)/shard_map/finish/pallas_call | solution.py:391
  (11 shorter events, 0.1 us)
Async XLA Ops:
  6.5 27.8 %copy-start.6 = (f32[2048]{0:T(1024)S(1)}, f32[2048]{0:T(1024)}, u32[]{:S(2)}) copy-start(f32[2048]{0:T(1024)} %param.21) | copy-start | bytes 24580
  6.5 27.8 %copy-start = (bf16[2048,256]{1,0:T(8,128)(2,1)S(1)}, bf16[2048,256]{1,0:T(8,128)(2,1)}, u32[]{:S(2)}) copy-start(bf16[2048,256]{1,0:T(8,128)(2,1)} %refs_0_.5) | copy-start | bytes 3145732
  6.5 27.8 %copy-start.1 = (bf16[2048,256]{1,0:T(8,128)(2,1)S(1)}, bf16[2048,256]{1,0:T(8,128)(2,1)}, u32[]{:S(2)}) copy-start(bf16[2048,256]{1,0:T(8,128)(2,1)} %refs_1_.5) | copy-start | bytes 3145732
  6.5 37.3 %copy-start.4 = (bf16[2048,256]{1,0:T(8,128)(2,1)S(1)}, bf16[2048,256]{1,0:T(8,128)(2,1)}, u32[]{:S(2)}) copy-start(bf16[2048,256]{1,0:T(8,128)(2,1)} %refs_2_.3) | copy-start | bytes 3145732
  6.5 37.3 %all-gather.3.cloned.1.call-start = ((), (), s32[]{:S(2)}) async-start(), calls=%async_computation.3 | async-start | bytes 4718592 | tf_op jit(solution)/shard_map/all_gather | solution.py:439
  7.3 97.6 %all-gather.5.cloned.1.call-start = ((), (), s32[]{:S(2)}) async-start(), calls=%async_computation.4 | async-start | bytes 9437184 | tf_op jit(solution)/shard_map/all_gather | solution.py:442
  9.3 14.2 %all-to-all-start = ((f32[16,8,256]{2,1,0:T(8,128)}), f32[16,8,256]{2,1,0:T(8,128)S(1)}, u32[]{:S(2)}, u32[]{:S(2)}) async-start(f32[16,8,256]{2,1,0:T(8,128)} %modulation_parts.1), calls=%async_computation | async-start | bytes 262144 | tf_op jit(solution)/shard_map/all_to_all | solution.py:444
  19.0 1.2 %copy-start.2 = (f32[2,256,896]{2,1,0:T(8,128)}, f32[2,256,896]{2,1,0:T(8,128)S(1)}, u32[]{:S(2)}) copy-start(f32[2,256,896]{2,1,0:T(8,128)S(1)} %bias_table.1.table_ref) | copy-start | bytes 5505028
  34.3 1.1 copy-start.5
  36.1 11.7 %collective-permute-start = (bf16[2,64,512]{2,1,0:T(8,128)(2,1)S(1)}, bf16[2,64,512]{2,1,0:T(8,128)(2,1)S(1)}, u32[]{:S(2)}, u32[]{:S(2)}) collective-permute-start(bf16[2,64,512]{2,1,0:T(8,128)(2,1)S(1)} %bitcast.12), channel_id=1, source_target_pairs={{0,8},{8,16},{16,24},{24,0},{32,40},{40,48},{48,56},{56,32},{64,72... | collective-permute-start | bytes 393224 | tf_op jit(solution)/shard_map/ppermute | solution.py:414
  36.7 11.2 %collective-permute-start.1 = (bf16[2,64,512]{2,1,0:T(8,128)(2,1)S(1)}, bf16[2,64,512]{2,1,0:T(8,128)(2,1)}, u32[]{:S(2)}, u32[]{:S(2)}) collective-permute-start(bf16[2,64,512]{2,1,0:T(8,128)(2,1)S(1)} %bitcast.13), channel_id=1, source_target_pairs={{0,16},{8,24},{16,0},{24,8},{32,48},{40,56},{48,32},{56,40},{64,80... | collective-permute-start | bytes 393224 | tf_op jit(solution)/shard_map/ppermute | solution.py:414
  38.8 9.0 %collective-permute-start.2 = (bf16[2,64,512]{2,1,0:T(8,128)(2,1)S(1)}, bf16[2,64,512]{2,1,0:T(8,128)(2,1)}, u32[]{:S(2)}, u32[]{:S(2)}) collective-permute-start(bf16[2,64,512]{2,1,0:T(8,128)(2,1)S(1)} %bitcast.14), channel_id=1, source_target_pairs={{0,24},{8,0},{16,8},{24,16},{32,56},{40,32},{48,40},{56,48},{64,88... | collective-permute-start | bytes 393224 | tf_op jit(solution)/shard_map/ppermute | solution.py:414
  48.9 27.6 %copy-start.3 = (f32[2,256,896]{2,1,0:T(8,128)S(1)}, f32[2,256,896]{2,1,0:T(8,128)}, u32[]{:S(2)}) copy-start(f32[2,256,896]{2,1,0:T(8,128)} %copy-done.2) | copy-start | bytes 5505028
  48.9 25.4 %collective-permute-start.3 = (bf16[4,2,64,512]{3,2,1,0:T(8,128)(2,1)S(1)}, bf16[4,2,64,512]{3,2,1,0:T(8,128)(2,1)S(1)}, u32[]{:S(2)}, u32[]{:S(2)}) collective-permute-start(bf16[4,2,64,512]{3,2,1,0:T(8,128)(2,1)S(1)} %pad_maximum_fusion.refs_0_), channel_id=1, source_target_pairs={{0,32},{8,40},{16,48},{24,56},{32,64},{40,72},{48,80},{56,88},{64,... | collective-permute-start | bytes 1572872 | tf_op jit(solution)/shard_map/ppermute | solution.py:471
  50.5 25.4 %collective-permute-start.4 = (bf16[4,2,64,512]{3,2,1,0:T(8,128)(2,1)S(1)}, bf16[4,2,64,512]{3,2,1,0:T(8,128)(2,1)S(1)}, u32[]{:S(2)}, u32[]{:S(2)}) collective-permute-start(bf16[4,2,64,512]{3,2,1,0:T(8,128)(2,1)S(1)} %pad_maximum_fusion.refs_0_), channel_id=1, source_target_pairs={{0,96},{8,104},{16,112},{24,120},{32,0},{40,8},{48,16},{56,24},{64... | collective-permute-start | bytes 1572872 | tf_op jit(solution)/shard_map/ppermute | solution.py:472
  54.9 28.5 %copy-start.7 = (f32[4]{0:T(128)S(1)}, f32[4]{0:T(128)}, u32[]{:S(2)}) copy-start(f32[4]{0:T(128)} %refs_5_.1) | copy-start | bytes 52
  54.9 21.5 %collective-permute-start.7 = (bf16[2,256,512]{2,1,0:T(8,128)(2,1)S(1)}, bf16[2,256,512]{2,1,0:T(8,128)(2,1)S(1)}, u32[]{:S(2)}, u32[]{:S(2)}) collective-permute-start(bf16[2,256,512]{2,1,0:T(8,128)(2,1)S(1)} %get-tuple-element.43), channel_id=1, source_target_pairs={{0,8},{8,16},{16,24},{24,32},{32,40},{40,48},{48,56},{56,64},{64,7... | collective-permute-start | bytes 1572872 | tf_op jit(solution)/shard_map/ppermute | solution.py:476
  58.3 18.2 %collective-permute-start.8 = (bf16[2,192,512]{2,1,0:T(8,128)(2,1)S(1)}, bf16[2,192,512]{2,1,0:T(8,128)(2,1)S(1)}, u32[]{:S(2)}, u32[]{:S(2)}) collective-permute-start(bf16[2,192,512]{2,1,0:T(8,128)(2,1)S(1)} %get-tuple-element.45), channel_id=1, source_target_pairs={{8,0},{16,8},{24,16},{32,24},{40,32},{48,40},{56,48},{64,56},{72,6... | collective-permute-start | bytes 1179656 | tf_op jit(solution)/shard_map/ppermute | solution.py:477
  74.3 7.8 %collective-permute-start.5 = (bf16[2,2,64,512]{3,2,1,0:T(8,128)(2,1)S(1)}, bf16[2,2,64,512]{3,2,1,0:T(8,128)(2,1)S(1)}, u32[]{:S(2)}, u32[]{:S(2)}) collective-permute-start(bf16[2,2,64,512]{3,2,1,0:T(8,128)(2,1)S(1)} %slice.8), channel_id=1, source_target_pairs={{0,32},{8,40},{16,48},{24,56},{32,64},{40,72},{48,80},{56,88},{64,... | collective-permute-start | bytes 786440 | tf_op jit(solution)/shard_map/ppermute | solution.py:483
  75.9 7.5 %collective-permute-start.6 = (bf16[2,2,64,512]{3,2,1,0:T(8,128)(2,1)S(1)}, bf16[2,2,64,512]{3,2,1,0:T(8,128)(2,1)S(1)}, u32[]{:S(2)}, u32[]{:S(2)}) collective-permute-start(bf16[2,2,64,512]{3,2,1,0:T(8,128)(2,1)S(1)} %slice.9), channel_id=1, source_target_pairs={{0,96},{8,104},{16,112},{24,120},{32,0},{40,8},{48,16},{56,24},{64... | collective-permute-start | bytes 786440 | tf_op jit(solution)/shard_map/ppermute | solution.py:484
Sparse Core Ops, SparseCore 0:
  9.0 34.7 all-gather.2
  45.6 49.6 all-gather.4
where the time goes:
time: 119 us; the launch traced here: 117 us
  Pallas kernels  30.4 us (26%)
  starting transfers between devices  24.5 us (21%)
  blocking collectives  24.2 us (20%)
  waiting for transfers between devices  20.5 us (17%)
  between operations  13.6 us (11%)
  local copies, waits for them, and re-layouts  3.15 us (3%)
    all_to_all x1, blocking collectives, computation(): attended = lax.all_to_all(attended, 'tp', 0, 0, tiled=True)  13.4 us
    ppermute x1, waiting for transfers between devices, computation(): below = lax.ppermute(ctx_line, 'sp', shifted(sp_size, 4, 4, 1))  11.2 us
    all_to_all x1, blocking collectives, copy_for_each(): lax.all_to_all(jnp.broadcast_to(shard[None], (length, *shard.shape)), axi...  10.8 us
    pallas_call x3, Pallas kernels, project(): pl.pallas_call(body, grid=(len(chosen), steps), in_specs=[blocks(width),...  8.48 us
    pallas_call x1, Pallas kernels, attend_far(): pl.pallas_call(body, grid=(samples, rows_dev // per), in_specs=[rows_spec...  7.99 us
    all_to_all x1, starting transfers between devices, computation(): summed = jnp.sum(lax.all_to_all(parts, 'sp', 0, 0, tiled=True), axis=0)  7.91 us
    pallas_call x1, Pallas kernels, finish(): pl.pallas_call(body, grid=(width // block,), in_specs=[whole(attended.sha...  5.78 us
    pallas_call x1, Pallas kernels, attend_near(): pl.pallas_call(body, grid=(samples, rows_dev // per), in_specs=[pl.BlockS...  5.24 us
  transfers between devices with their start and end apart: 12, of which 5 were waited for; matrix products, arithmetic and copies ran while one was open for 2% of the time, Pallas kernels for 21%

commit v1 on v0

--- a/solution.py
+++ b/solution.py
@@ -216,7 +216,7 @@
     return [gather_heads(array, masks) for array in (mixed, top, total)]
 
 
-def attend_near(place, query, before, pair, after, table, rows_all, per):
+def attend_near(place, query, before, pair, after, table, far, rows_all, per):
     samples, tokens, cols = query.shape
     rows_dev = tokens // GRID_W
     near_keys = WIN_ROWS * GRID_W
@@ -226,7 +226,7 @@
     bf16, f32 = jnp.bfloat16, jnp.float32
 
     def body(place_ref, q_ref, before_ref, pair_ref, after_ref, table_ref, *refs):
-        out_refs, (near_t, values) = refs[:3], refs[3:]
+        mixed_ref, top_ref, total_ref, out_ref, near_t, values = refs
         sample, step = pl.program_id(0), pl.program_id(1)
 
         @pl.when(step == 0)
@@ -270,8 +270,15 @@
             starts.append(pl.multiple_of(local * GRID_W, GRID_W))
         for r in range(per):
             parts = weighed(scores[r], values[pl.ds(starts[r], near_keys), :], masks)
-            for out_ref, part in zip(out_refs, parts):
-                out_ref[0, r * GRID_W : (r + 1) * GRID_W] = part
+            mixed, top, total = parts
+            at = slice(r * GRID_W, (r + 1) * GRID_W)
+            far_top = top_ref[0, at]
+            highest = jnp.maximum(top, far_top)
+            near_part = jnp.exp(top - highest)
+            far_part = jnp.exp(far_top - highest)
+            total = total * near_part + total_ref[0, at] * far_part
+            mixed = mixed * near_part + mixed_ref[0, at] * far_part
+            out_ref[r, 0] = (mixed / total).astype(bf16)
 
     def of_sample(array):
         return pl.BlockSpec((1, *array.shape[1:]), lambda s, i: (s, 0, 0))
@@ -287,19 +294,20 @@
             of_sample(pair),
             RESIDENT,
             RESIDENT,
-        ],
-        out_specs=[rows_spec] * 3,
-        out_shape=[jax.ShapeDtypeStruct((samples, tokens, cols), f32)] * 3,
+        ]
+        + [rows_spec] * 3,
+        out_specs=pl.BlockSpec((per, 1, GRID_W, cols), lambda s, i: (i, s, 0, 0)),
+        out_shape=jax.ShapeDtypeStruct((rows_dev, samples, GRID_W, cols), bf16),
         scratch_shapes=[
             pltpu.VMEM((2, cols, lanes), bf16),
             pltpu.VMEM((padded, cols), bf16),
         ],
         compiler_params=pltpu.CompilerParams(vmem_limit_bytes=32 * 2**20),
         name="attend_near",
-    )(place, query, before, pair, after, table)
-
-
-def attend_far(query, ctx_pairs, ctx_bias, near, per):
+    )(place, query, before, pair, after, table, *far)
+
+
+def attend_far(query, ctx_pairs, ctx_bias, per):
     samples, tokens, cols = query.shape
     rows_dev = tokens // GRID_W
     ctx_rows = ctx_pairs[0].shape[2]
@@ -309,7 +317,7 @@
 
     def body(q_ref, *refs):
         ctx_refs = refs[: len(members)]
-        cb_ref, mixed_ref, top_ref, total_ref, out_ref, far_t, values = refs[len(members) :]
+        cb_ref, *out_refs, far_t, values = refs[len(members) :]
         sample, step = pl.program_id(0), pl.program_id(1)
 
         @pl.when(step == 0)
@@ -340,15 +348,9 @@
         ]
         for r in range(per):
             mixed, top, total = weighed(scores[r], values[...], masks)
-            at = slice(r * GRID_W, (r + 1) * GRID_W)
             top = top + gather_heads(context_bias, masks)
-            near_top = top_ref[0, at]
-            highest = jnp.maximum(top, near_top)
-            far_part = jnp.exp(top - highest)
-            near_part = jnp.exp(near_top - highest)
-            total = total * far_part + total_ref[0, at] * near_part
-            mixed = mixed * far_part + mixed_ref[0, at] * near_part
-            out_ref[r, 0] = (mixed / total).astype(bf16)
+            for out_ref, part in zip(out_refs, (mixed, top, total)):
+                out_ref[0, r * GRID_W : (r + 1) * GRID_W] = part
 
     rows_spec = pl.BlockSpec((1, per * GRID_W, cols), lambda s, i: (s, i, 0))
     return pl.pallas_call(
@@ -358,17 +360,16 @@
             rows_spec,
         ]
         + [RESIDENT] * len(members)
-        + [pl.BlockSpec(memory_space=pltpu.SMEM)]
-        + [rows_spec] * 3,
-        out_specs=pl.BlockSpec((per, 1, GRID_W, cols), lambda s, i: (i, s, 0, 0)),
-        out_shape=jax.ShapeDtypeStruct((rows_dev, samples, GRID_W, cols), bf16),
+        + [pl.BlockSpec(memory_space=pltpu.SMEM)],
+        out_specs=[rows_spec] * 3,
+        out_shape=[jax.ShapeDtypeStruct((samples, tokens, cols), f32)] * 3,
         scratch_shapes=[
             pltpu.VMEM((cols, ctx_count), bf16),
             pltpu.VMEM((ctx_count, cols), bf16),
         ],
         compiler_params=pltpu.CompilerParams(vmem_limit_bytes=32 * 2**20),
         name="attend_far",
-    )(query, *ctx_pairs, ctx_bias, *near)
+    )(query, *ctx_pairs, ctx_bias)
 
 
 def finish(attended, w_out, latent, modulation, tiles):
@@ -473,19 +474,23 @@
     for s in range(1, samples):
         outs = project(gathered, gain, modulation, w_triple, 0, 256, ends, s, outs)
     pair, query, first, last = outs
-    before = resident(lax.ppermute(last, "sp", up))
-    after = resident(lax.ppermute(first, "sp", down))
     rows_all = pair.shape[1] // GRID_W * sp_size
+    column = sp_index % 4
+    rest = list(zip(shifted(sp_size, 4, 4, 1), shifted(sp_size, 4, 4, 3)))
+    one_way = [down if i % 4 == 0 else up for i, (up, down) in enumerate(rest)]
+    other_way = [up if i % 4 == 3 else down for i, (up, down) in enumerate(rest)]
     ctx_pairs = [
         ctx_line,
         below,
         above,
-        lax.ppermute(below[:2], "sp", shifted(sp_size, 4, 4, 1)),
-        lax.ppermute(above[2:], "sp", shifted(sp_size, 4, 4, 3)),
+        lax.ppermute(jnp.where(column == 0, above[:2], below[:2]), "sp", one_way),
+        lax.ppermute(jnp.where(column == 3, below[2:], above[2:]), "sp", other_way),
     ]
+    before = resident(lax.ppermute(last, "sp", up))
+    after = resident(lax.ppermute(first, "sp", down))
     ctx_pairs = [resident(array) for array in ctx_pairs]
-    near = attend_near(place, query, before, pair, after, table, rows_all, 4)
-    attended = attend_far(query, ctx_pairs, ctx_bias, near, 4)
+    far = attend_far(query, ctx_pairs, ctx_bias, 4)
+    attended = attend_near(place, query, before, pair, after, table, far, rows_all, 4)
     attended = attended.reshape(tp_size, samples * tokens_dev, local_cols)
     attended = lax.all_to_all(attended, "tp", 0, 0, tiled=True)
     return finish(attended, w_out_all, latent, modulation, 4)

time: 119 us -> 125 us (1.050)
  Pallas kernels: 30.4 us -> 33.2 us
  waiting for transfers between devices: 20.5 us -> 18.5 us
  local copies, waits for them, and re-layouts: 3.15 us -> 5.08 us
  starting transfers between devices: 24.5 us -> 26 us
    ppermute x1, waiting for transfers between devices: 11.2 us -> 0.01 us  [computation(): below = lax.ppermute(ctx_line, 'sp', shifted(sp_size, 4, 4, 1))]
    ppermute x2, waiting for transfers between devices: 1.69 us -> 9.67 us  [the longest x1 5.76 us: computation(): lax.ppermute(jnp.where(column == 0, above[:2], below[:2]), 'sp', one_way)]
    unnamed x17 -> x23, local copies, waits for them, and re-layouts: 3.1 us -> 5.07 us
    pallas_call x3, Pallas kernels: 8.48 us -> 9.84 us  [project(): pl.pallas_call(body, grid=(len(chosen), steps), in_specs=[blocks(width),...]
    ppermute x2, starting transfers between devices: 2.16 us -> 3.48 us  [the longest x1 3.41 us: computation(): lax.ppermute(jnp.where(column == 3, below[2:], above[2:]), 'sp', other_way)]
  transfers between devices with their start and end apart: 12 -> 12, of which waited for: 5 -> 4; matrix products, arithmetic and copies ran while one was open for 2% -> 2% of each run, Pallas kernels for 21% -> 22%
where the time goes in v1:
time: 125 us; the launch traced here: 123 us
  Pallas kernels  33.2 us (27%)
  starting transfers between devices  26 us (21%)
  blocking collectives  24.2 us (19%)
  waiting for transfers between devices  18.5 us (15%)
  between operations  13.6 us (11%)
  local copies, waits for them, and re-layouts  5.08 us (4%)
  other arithmetic  2.3 us (2%)
    all_to_all x1, blocking collectives, computation(): attended = lax.all_to_all(attended, 'tp', 0, 0, tiled=True)  13.4 us
    all_to_all x1, blocking collectives, copy_for_each(): lax.all_to_all(jnp.broadcast_to(shard[None], (length, *shard.shape)), axi...  10.8 us
    pallas_call x3, Pallas kernels, project(): pl.pallas_call(body, grid=(len(chosen), steps), in_specs=[blocks(width),...  9.84 us
    pallas_call x1, Pallas kernels, attend_far(): pl.pallas_call(body, grid=(samples, rows_dev // per), in_specs=[rows_spec...  8.38 us
    all_to_all x1, starting transfers between devices, computation(): summed = jnp.sum(lax.all_to_all(parts, 'sp', 0, 0, tiled=True), axis=0)  7.91 us
    pallas_call x1, Pallas kernels, attend_near(): pl.pallas_call(body, grid=(samples, rows_dev // per), in_specs=[pl.BlockS...  6.42 us
    pallas_call x1, Pallas kernels, finish(): pl.pallas_call(body, grid=(width // block,), in_specs=[whole(attended.sha...  5.79 us
    ppermute x1, waiting for transfers between devices, computation(): lax.ppermute(jnp.where(column == 0, above[:2], below[:2]), 'sp', one_way)  5.76 us
  transfers between devices with their start and end apart: 12, of which 4 were waited for; matrix products, arithmetic and copies ran while one was open for 2% of the time, Pallas kernels for 22%

profile of v1, /device:TPU:32, one launch (start us, length us, event | category | flops | bytes accessed | tf_op | source)
XLA Modules:
  0.0 122.9 jit_solution(15111436863129463575)
XLA Ops:
  6.5 0.0 all-gather.3.cloned.1.call-start
  6.6 0.7 all-gather.3.cloned.1.call-update
  7.3 0.0 all-gather.5.cloned.1.call-start
  7.3 1.8 %modulation_parts.1 = f32[16,8,256]{2,1,0:T(8,128)} custom-call(s32[1]{0:T(128)} %bitcast.place_ref, bf16[2,2048]{1,0:T(2,128)(2,1)} %cond_ref.1, bf16[2048]{0:T(1024)(128)(2,1)} %ctx_ref.1, bf16[128,256]{1,0:T(8,128)(2,1)} %shift_ref.1, bf16[128,256]{1,0:T(8,128)(2,1)} %scale_ref.1, bf16[128,256]{1,0:T(8,128)(2,1)} %gate_ref.1), custom_call_target="tpu_custom_call" | custom-call | tf_op jit(solution)/shard_map/modulation_parts/pallas_call | solution.py:53
  9.1 0.0 all-gather.5.cloned.1.call-update
  9.1 7.9 %all-to-all-start = ((f32[16,8,256]{2,1,0:T(8,128)}), f32[16,8,256]{2,1,0:T(8,128)S(1)}, u32[]{:S(2)}, u32[]{:S(2)}) async-start(f32[16,8,256]{2,1,0:T(8,128)} %modulation_parts.1), calls=%async_computation | async-start | bytes 262144 | tf_op jit(solution)/shard_map/all_to_all | solution.py:445
  17.1 0.8 copy.20
  17.8 1.0 bias_table.1.table_ref
  18.8 0.0 copy-start.2
  18.8 1.2 %copy-done.2 = f32[2,256,896]{2,1,0:T(8,128)} copy-done((f32[2,256,896]{2,1,0:T(8,128)}, f32[2,256,896]{2,1,0:T(8,128)S(1)}, u32[]{:S(2)}) %copy-start.2) | copy-done | bytes 1835032
  20.1 3.3 %all-to-all-done = f32[16,8,256]{2,1,0:T(8,128)S(1)} async-done(((f32[16,8,256]{2,1,0:T(8,128)}), f32[16,8,256]{2,1,0:T(8,128)S(1)}, u32[]{:S(2)}, u32[]{:S(2)}) %all-to-all-start) | async-done | bytes 131104 | tf_op jit(solution)/shard_map/all_to_all | solution.py:445
  23.4 10.8 %all_to_all.15.tiles_ref.tile_ref = f32[8,8,256]{2,1,0:T(8,128)S(1)} all-to-all(f32[8,8,256]{2,1,0:T(8,128)S(1)} %broadcast_in_dim.14), channel_id=1, replica_groups=mesh['sp'=16,'tp'=8] {'tp'}, dimensions={0} | all-to-all | bytes 131072 | tf_op jit(solution)/shard_map/all_to_all | solution.py:22
  34.2 0.0 copy-done.9
  34.2 0.0 copy-done
  34.2 0.0 copy-done.1
  34.2 0.0 copy-done.7
  34.2 0.6 project.3
  34.9 0.6 collective-permute-start
  35.5 2.2 %collective-permute-start.1 = (bf16[2,64,512]{2,1,0:T(8,128)(2,1)S(1)}, bf16[2,64,512]{2,1,0:T(8,128)(2,1)}, u32[]{:S(2)}, u32[]{:S(2)}) collective-permute-start(bf16[2,64,512]{2,1,0:T(8,128)(2,1)S(1)} %bitcast.13), channel_id=1, source_target_pairs={{0,16},{8,24},{16,0},{24,8},{32,48},{40,56},{48,32},{56,40},{64,80... | collective-permute-start | bytes 393224 | tf_op jit(solution)/shard_map/ppermute | solution.py:415
  37.6 1.4 %collective-permute-start.2 = (bf16[2,64,512]{2,1,0:T(8,128)(2,1)S(1)}, bf16[2,64,512]{2,1,0:T(8,128)(2,1)}, u32[]{:S(2)}, u32[]{:S(2)}) collective-permute-start(bf16[2,64,512]{2,1,0:T(8,128)(2,1)S(1)} %bitcast.14), channel_id=1, source_target_pairs={{0,24},{8,0},{16,8},{24,16},{32,56},{40,32},{48,40},{56,48},{64,88... | collective-permute-start | bytes 393224 | tf_op jit(solution)/shard_map/ppermute | solution.py:415
  39.1 4.8 %all-gather.3.cloned.1.call-done.rows_ref = bf16[2,512,2048]{2,1,0:T(8,128)(2,1)} async-done(((bf16[2,64,2048]{2,1,0:T(8,128)(2,1)}), bf16[2,512,2048]{2,1,0:T(8,128)(2,1)}) %all-gather.3.cloned.1.call-update) | async-done | bytes 4194320 | tf_op jit(solution)/shard_map/all_gather | solution.py:440
  43.9 1.2 copy-done.6
  45.1 4.6 %project.4 = (bf16[2,512,512]{2,1,0:T(8,128)(2,1)S(1)}, bf16[2,512,256]{2,1,0:T(8,128)(2,1)S(1)}, bf16[2,192,512]{2,1,0:T(8,128)(2,1)S(1)}, bf16[2,256,512]{2,1,0:T(8,128)(2,1)}) custom-call(bf16[2,512,2048]{2,1,0:T(8,128)(2,1)} %all-gather.3.cloned.1.call-done.rows_ref, f32[1,2048]{1,0:T(1,128)S(1)} %bitcast.18, ...), custom_call_target="tpu_custom_call" | custom-call | tf_op jit(solution)/shard_map/project/pallas_call | solution.py:141
  49.7 0.0 collective-permute-done
  49.7 0.0 collective-permute-done.1
  49.7 0.0 collective-permute-done.2
  49.7 1.0 pad_maximum_fusion.refs_0_
  50.7 0.0 copy-start.10
  50.7 1.6 %collective-permute-start.5 = (bf16[4,2,64,512]{3,2,1,0:T(8,128)(2,1)S(1)}, bf16[4,2,64,512]{3,2,1,0:T(8,128)(2,1)}, u32[]{:S(2)}, u32[]{:S(2)}) collective-permute-start(bf16[4,2,64,512]{3,2,1,0:T(8,128)(2,1)S(1)} %pad_maximum_fusion.refs_0_), channel_id=1, source_target_pairs={{0,32},{8,40},{16,48},{24,56},{32,64},{40,72},{48,80},{56,88},{64,... | collective-permute-start | bytes 1572872 | tf_op jit(solution)/shard_map/ppermute | solution.py:472
  52.4 0.5 collective-permute-start.6
  52.8 4.6 %project.5 = (bf16[2,512,512]{2,1,0:T(8,128)(2,1)S(1)}, bf16[2,512,256]{2,1,0:T(8,128)(2,1)S(1)}, bf16[2,192,512]{2,1,0:T(8,128)(2,1)S(1)}, bf16[2,256,512]{2,1,0:T(8,128)(2,1)}) custom-call(bf16[2,512,2048]{2,1,0:T(8,128)(2,1)} %all-gather.3.cloned.1.call-done.rows_ref, ...), custom_call_target="tpu_custom_call", output_to_operand_aliasing={{0}: (6, {}), {1}: (7, {}), {2}: (8, {}), {3}: (9, {})} | custom-call | tf_op jit(solution)/shard_map/project/pallas_call | solution.py:141
  57.4 1.0 copy-done.4
  58.5 0.8 copy-done.8
  59.3 3.5 %collective-permute-start.3 = (bf16[2,256,512]{2,1,0:T(8,128)(2,1)}, bf16[2,256,512]{2,1,0:T(8,128)(2,1)}, u32[]{:S(2)}, u32[]{:S(2)}) collective-permute-start(bf16[2,256,512]{2,1,0:T(8,128)(2,1)} %get-tuple-element.39), channel_id=1, source_target_pairs={{0,8},{8,16},{16,24},{24,32},{32,40},{40,48},{48,56},{56,64},{64,7... | collective-permute-start | bytes 1572872 | tf_op jit(solution)/shard_map/ppermute | solution.py:489
  62.8 4.7 %collective-permute-start.4 = (bf16[2,192,512]{2,1,0:T(8,128)(2,1)}, bf16[2,192,512]{2,1,0:T(8,128)(2,1)S(1)}, u32[]{:S(2)}, u32[]{:S(2)}) collective-permute-start(bf16[2,192,512]{2,1,0:T(8,128)(2,1)} %copy-done.8), channel_id=1, source_target_pairs={{8,0},{16,8},{24,16},{32,24},{40,32},{48,40},{56,48},{64,56},{72,6... | collective-permute-start | bytes 1179656 | tf_op jit(solution)/shard_map/ppermute | solution.py:490
  67.5 0.0 collective-permute-done.5.refs_1_
  67.5 0.0 collective-permute-done.6.refs_2_
  67.5 1.2 %slice_select_fusion = (bf16[2,2,64,512]{3,2,1,0:T(8,128)(2,1)S(1)}, bf16[2,2,64,512]{3,2,1,0:T(8,128)(2,1)S(1)}) fusion(bf16[4,2,64,512]{3,2,1,0:T(8,128)(2,1)} %collective-permute-done.6.refs_2_, bf16[4,2,64,512]{3,2,1,0:T(8,128)(2,1)} %collective-permute-done.5.refs_1_, pred[]{:T(512)S(6)} %eq.9, pred[]{:T(512)S(6)} %eq.8), kind=kLoop, calls=%fused_computation.1 | loop fusion | flops 262144 | bytes 1572866 | tf_op jit(solution)/shard_map/jit(_where)/select_n | solution.py:487
  68.8 0.1 collective-permute-start.7
  68.9 3.4 %collective-permute-start.8 = (bf16[2,2,64,512]{3,2,1,0:T(8,128)(2,1)S(1)}, bf16[2,2,64,512]{3,2,1,0:T(8,128)(2,1)S(1)}, u32[]{:S(2)}, u32[]{:S(2)}) collective-permute-start(bf16[2,2,64,512]{3,2,1,0:T(8,128)(2,1)S(1)} %get-tuple-element.51), channel_id=1, source_target_pairs={{0,96},{8,104},{16,112},{24,56},{32,0},{40,8},{48,16},{56,88},{64,... | collective-permute-start | bytes 786440 | tf_op jit(solution)/shard_map/ppermute | solution.py:487
  72.3 5.8 %collective-permute-done.7.refs_3_ = bf16[2,2,64,512]{3,2,1,0:T(8,128)(2,1)S(1)} collective-permute-done((bf16[2,2,64,512]{3,2,1,0:T(8,128)(2,1)S(1)}, bf16[2,2,64,512]{3,2,1,0:T(8,128)(2,1)S(1)}, u32[]{:S(2)}, u32[]{:S(2)}) %collective-permute-start.7) | collective-permute-done | bytes 262176 | tf_op jit(solution)/shard_map/ppermute | solution.py:486
  78.0 3.9 %collective-permute-done.8.refs_4_ = bf16[2,2,64,512]{3,2,1,0:T(8,128)(2,1)S(1)} collective-permute-done((bf16[2,2,64,512]{3,2,1,0:T(8,128)(2,1)S(1)}, bf16[2,2,64,512]{3,2,1,0:T(8,128)(2,1)S(1)}, u32[]{:S(2)}, u32[]{:S(2)}) %collective-permute-start.8) | collective-permute-done | bytes 262176 | tf_op jit(solution)/shard_map/ppermute | solution.py:487
  81.9 8.4 %attend_far.1 = (f32[2,512,256]{2,1,0:T(8,128)S(1)}, f32[2,512,256]{2,1,0:T(8,128)S(1)}, f32[2,512,256]{2,1,0:T(8,128)S(1)}) custom-call(bf16[2,512,256]{2,1,0:T(8,128)(2,1)S(1)} %get-tuple-element.38.q_ref, bf16[4,2,64,512]{3,2,1,0:T(8,128)(2,1)S(1)} %pad_maximum_fusion.refs_0_, bf16[4,2,64,512]{3,2,1,0:T(8,128)(2,1)} %collective-permute-done.5.refs_1_, ...), custom_call_target="tpu_custom_call" | custom-call | tf_op jit(solution)/shard_map/attend_far/pallas_call | solution.py:356
  90.3 0.0 collective-permute-done.4.after_ref
  90.3 0.0 collective-permute-done.3.before_ref
  90.4 6.4 %attend_near.1 = bf16[8,2,64,256]{3,2,1,0:T(8,128)(2,1)S(1)} custom-call(s32[1]{0:T(128)} %bitcast.place_ref, bf16[2,512,256]{2,1,0:T(8,128)(2,1)S(1)} %get-tuple-element.38.q_ref, bf16[2,256,512]{2,1,0:T(8,128)(2,1)} %collective-permute-done.3.before_ref, bf16[2,512,512]{2,1,0:T(8,128)(2,1)S(1)} %copy-done.5, ...), custom_call_target="tpu_custom_call" | custom-call | tf_op jit(solution)/shard_map/attend_near/pallas_call | solution.py:287
  96.8 13.4 %all_to_all.16.att_ref = bf16[8,128,256]{2,1,0:T(8,128)(2,1)} all-to-all(bf16[8,128,256]{2,1,0:T(8,128)(2,1)S(1)} %bitcast.10), channel_id=1, replica_groups=mesh['sp'=16,'tp'=8] {'tp'}, dimensions={0} | all-to-all | bytes 1048576 | tf_op jit(solution)/shard_map/all_to_all | solution.py:495
  110.2 5.8 %finish.1 = bf16[2,64,2048]{2,1,0:T(8,128)(2,1)} custom-call(bf16[8,128,256]{2,1,0:T(8,128)(2,1)} %all_to_all.16.att_ref, bf16[2048,2048]{1,0:T(8,128)(2,1)} %all-gather.5.cloned.1.call-done.w_ref, bf16[2,64,2048]{2,1,0:T(8,128)(2,1)} %latent_ref.1, f32[8,8,256]{2,1,0:T(8,128)S(1)} %all_to_all.15.tiles_ref.tile_ref), custom_call_target="tpu_custom_call" | custom-call | tf_op jit(solution)/shard_map/finish/pallas_call | solution.py:392
  (16 shorter events, 0.1 us)
Async XLA Ops:
  6.5 27.7 %copy-start.9 = (f32[2048]{0:T(1024)S(1)}, f32[2048]{0:T(1024)}, u32[]{:S(2)}) copy-start(f32[2048]{0:T(1024)} %param.21) | copy-start | bytes 24580
  6.5 27.7 %copy-start = (bf16[2048,256]{1,0:T(8,128)(2,1)S(1)}, bf16[2048,256]{1,0:T(8,128)(2,1)}, u32[]{:S(2)}) copy-start(bf16[2048,256]{1,0:T(8,128)(2,1)} %refs_0_.5) | copy-start | bytes 3145732
  6.5 27.7 %copy-start.1 = (bf16[2048,256]{1,0:T(8,128)(2,1)S(1)}, bf16[2048,256]{1,0:T(8,128)(2,1)}, u32[]{:S(2)}) copy-start(bf16[2048,256]{1,0:T(8,128)(2,1)} %refs_1_.5) | copy-start | bytes 3145732
  6.5 27.7 %copy-start.7 = (bf16[2,64,2048]{2,1,0:T(8,128)(2,1)S(1)}, bf16[2,64,2048]{2,1,0:T(8,128)(2,1)}, u32[]{:S(2)}) copy-start(bf16[2,64,2048]{2,1,0:T(8,128)(2,1)} %param.15) | copy-start | bytes 1572868
  6.5 37.3 %all-gather.3.cloned.1.call-start = ((), (), s32[]{:S(2)}) async-start(), calls=%async_computation.3 | async-start | bytes 4718592 | tf_op jit(solution)/shard_map/all_gather | solution.py:440
  7.3 103.0 %all-gather.5.cloned.1.call-start = ((), (), s32[]{:S(2)}) async-start(), calls=%async_computation.4 | async-start | bytes 9437184 | tf_op jit(solution)/shard_map/all_gather | solution.py:443
  9.1 14.2 %all-to-all-start = ((f32[16,8,256]{2,1,0:T(8,128)}), f32[16,8,256]{2,1,0:T(8,128)S(1)}, u32[]{:S(2)}, u32[]{:S(2)}) async-start(f32[16,8,256]{2,1,0:T(8,128)} %modulation_parts.1), calls=%async_computation | async-start | bytes 262144 | tf_op jit(solution)/shard_map/all_to_all | solution.py:445
  18.8 1.2 %copy-start.2 = (f32[2,256,896]{2,1,0:T(8,128)}, f32[2,256,896]{2,1,0:T(8,128)S(1)}, u32[]{:S(2)}) copy-start(f32[2,256,896]{2,1,0:T(8,128)S(1)} %bias_table.1.table_ref) | copy-start | bytes 5505028
  34.9 14.8 %collective-permute-start = (bf16[2,64,512]{2,1,0:T(8,128)(2,1)S(1)}, bf16[2,64,512]{2,1,0:T(8,128)(2,1)S(1)}, u32[]{:S(2)}, u32[]{:S(2)}) collective-permute-start(bf16[2,64,512]{2,1,0:T(8,128)(2,1)S(1)} %bitcast.12), channel_id=1, source_target_pairs={{0,8},{8,16},{16,24},{24,0},{32,40},{40,48},{48,56},{56,32},{64,72... | collective-permute-start | bytes 393224 | tf_op jit(solution)/shard_map/ppermute | solution.py:415
  35.5 14.2 %collective-permute-start.1 = (bf16[2,64,512]{2,1,0:T(8,128)(2,1)S(1)}, bf16[2,64,512]{2,1,0:T(8,128)(2,1)}, u32[]{:S(2)}, u32[]{:S(2)}) collective-permute-start(bf16[2,64,512]{2,1,0:T(8,128)(2,1)S(1)} %bitcast.13), channel_id=1, source_target_pairs={{0,16},{8,24},{16,0},{24,8},{32,48},{40,56},{48,32},{56,40},{64,80... | collective-permute-start | bytes 393224 | tf_op jit(solution)/shard_map/ppermute | solution.py:415
  37.6 12.1 %collective-permute-start.2 = (bf16[2,64,512]{2,1,0:T(8,128)(2,1)S(1)}, bf16[2,64,512]{2,1,0:T(8,128)(2,1)}, u32[]{:S(2)}, u32[]{:S(2)}) collective-permute-start(bf16[2,64,512]{2,1,0:T(8,128)(2,1)S(1)} %bitcast.14), channel_id=1, source_target_pairs={{0,24},{8,0},{16,8},{24,16},{32,56},{40,32},{48,40},{56,48},{64,88... | collective-permute-start | bytes 393224 | tf_op jit(solution)/shard_map/ppermute | solution.py:415
  43.9 1.2 copy-start.6
  50.7 31.2 %copy-start.10 = (f32[4]{0:T(128)S(1)}, f32[4]{0:T(128)}, u32[]{:S(2)}) copy-start(f32[4]{0:T(128)} %refs_5_.1) | copy-start | bytes 52
  50.7 16.8 %collective-permute-start.5 = (bf16[4,2,64,512]{3,2,1,0:T(8,128)(2,1)S(1)}, bf16[4,2,64,512]{3,2,1,0:T(8,128)(2,1)}, u32[]{:S(2)}, u32[]{:S(2)}) collective-permute-start(bf16[4,2,64,512]{3,2,1,0:T(8,128)(2,1)S(1)} %pad_maximum_fusion.refs_0_), channel_id=1, source_target_pairs={{0,32},{8,40},{16,48},{24,56},{32,64},{40,72},{48,80},{56,88},{64,... | collective-permute-start | bytes 1572872 | tf_op jit(solution)/shard_map/ppermute | solution.py:472
  52.4 15.2 %collective-permute-start.6 = (bf16[4,2,64,512]{3,2,1,0:T(8,128)(2,1)S(1)}, bf16[4,2,64,512]{3,2,1,0:T(8,128)(2,1)}, u32[]{:S(2)}, u32[]{:S(2)}) collective-permute-start(bf16[4,2,64,512]{3,2,1,0:T(8,128)(2,1)S(1)} %pad_maximum_fusion.refs_0_), channel_id=1, source_target_pairs={{0,96},{8,104},{16,112},{24,120},{32,0},{40,8},{48,16},{56,24},{64... | collective-permute-start | bytes 1572872 | tf_op jit(solution)/shard_map/ppermute | solution.py:473
  57.4 1.0 copy-start.4
  58.5 0.8 copy-start.8
  59.3 31.1 %copy-start.3 = (f32[2,256,896]{2,1,0:T(8,128)S(1)}, f32[2,256,896]{2,1,0:T(8,128)}, u32[]{:S(2)}) copy-start(f32[2,256,896]{2,1,0:T(8,128)} %copy-done.2) | copy-start | bytes 5505028
  59.3 31.1 %collective-permute-start.3 = (bf16[2,256,512]{2,1,0:T(8,128)(2,1)}, bf16[2,256,512]{2,1,0:T(8,128)(2,1)}, u32[]{:S(2)}, u32[]{:S(2)}) collective-permute-start(bf16[2,256,512]{2,1,0:T(8,128)(2,1)} %get-tuple-element.39), channel_id=1, source_target_pairs={{0,8},{8,16},{16,24},{24,32},{32,40},{40,48},{48,56},{56,64},{64,7... | collective-permute-start | bytes 1572872 | tf_op jit(solution)/shard_map/ppermute | solution.py:489
  62.8 27.6 %copy-start.5 = (bf16[2,512,512]{2,1,0:T(8,128)(2,1)S(1)}, bf16[2,512,512]{2,1,0:T(8,128)(2,1)}, u32[]{:S(2)}) copy-start(bf16[2,512,512]{2,1,0:T(8,128)(2,1)} %copy-done.4) | copy-start | bytes 3145732
  62.8 27.5 %collective-permute-start.4 = (bf16[2,192,512]{2,1,0:T(8,128)(2,1)}, bf16[2,192,512]{2,1,0:T(8,128)(2,1)S(1)}, u32[]{:S(2)}, u32[]{:S(2)}) collective-permute-start(bf16[2,192,512]{2,1,0:T(8,128)(2,1)} %copy-done.8), channel_id=1, source_target_pairs={{8,0},{16,8},{24,16},{32,24},{40,32},{48,40},{56,48},{64,56},{72,6... | collective-permute-start | bytes 1179656 | tf_op jit(solution)/shard_map/ppermute | solution.py:490
  68.8 9.2 %collective-permute-start.7 = (bf16[2,2,64,512]{3,2,1,0:T(8,128)(2,1)S(1)}, bf16[2,2,64,512]{3,2,1,0:T(8,128)(2,1)S(1)}, u32[]{:S(2)}, u32[]{:S(2)}) collective-permute-start(bf16[2,2,64,512]{3,2,1,0:T(8,128)(2,1)S(1)} %get-tuple-element.52), channel_id=1, source_target_pairs={{0,96},{8,40},{16,48},{24,56},{32,0},{40,72},{48,80},{56,88},{64,3... | collective-permute-start | bytes 786440 | tf_op jit(solution)/shard_map/ppermute | solution.py:486
  68.9 13.1 %collective-permute-start.8 = (bf16[2,2,64,512]{3,2,1,0:T(8,128)(2,1)S(1)}, bf16[2,2,64,512]{3,2,1,0:T(8,128)(2,1)S(1)}, u32[]{:S(2)}, u32[]{:S(2)}) collective-permute-start(bf16[2,2,64,512]{3,2,1,0:T(8,128)(2,1)S(1)} %get-tuple-element.51), channel_id=1, source_target_pairs={{0,96},{8,104},{16,112},{24,56},{32,0},{40,8},{48,16},{56,88},{64,... | collective-permute-start | bytes 786440 | tf_op jit(solution)/shard_map/ppermute | solution.py:487
Sparse Core Ops, SparseCore 0:
  9.0 34.7 all-gather.2
  45.6 49.5 all-gather.4

commit v2 on v1

--- a/solution.py
+++ b/solution.py
@@ -475,16 +475,12 @@
         outs = project(gathered, gain, modulation, w_triple, 0, 256, ends, s, outs)
     pair, query, first, last = outs
     rows_all = pair.shape[1] // GRID_W * sp_size
-    column = sp_index % 4
-    rest = list(zip(shifted(sp_size, 4, 4, 1), shifted(sp_size, 4, 4, 3)))
-    one_way = [down if i % 4 == 0 else up for i, (up, down) in enumerate(rest)]
-    other_way = [up if i % 4 == 3 else down for i, (up, down) in enumerate(rest)]
     ctx_pairs = [
         ctx_line,
         below,
         above,
-        lax.ppermute(jnp.where(column == 0, above[:2], below[:2]), "sp", one_way),
-        lax.ppermute(jnp.where(column == 3, below[2:], above[2:]), "sp", other_way),
+        lax.ppermute(below[:2], "sp", shifted(sp_size, 4, 4, 1)),
+        lax.ppermute(above[2:], "sp", shifted(sp_size, 4, 4, 3)),
     ]
     before = resident(lax.ppermute(last, "sp", up))
     after = resident(lax.ppermute(first, "sp", down))

time: 125 us -> 124 us (level)
  waiting for transfers between devices: 18.5 us -> 25.8 us
  Pallas kernels: 33.2 us -> 30.7 us
  local copies, waits for them, and re-layouts: 5.08 us -> 3.15 us
  starting transfers between devices: 26 us -> 24.5 us
    ppermute x1, waiting for transfers between devices: 0.01 us -> 11.2 us  [computation(): below = lax.ppermute(ctx_line, 'sp', shifted(sp_size, 4, 4, 1))]
    ppermute x2, waiting for transfers between devices: 9.67 us -> 6.95 us  [the longest x1 5.58 us: computation(): lax.ppermute(below[:2], 'sp', shifted(sp_size, 4, 4, 1))]
    unnamed x23 -> x17, local copies, waits for them, and re-layouts: 5.07 us -> 3.1 us
    pallas_call x3, Pallas kernels: 9.84 us -> 8.47 us  [project(): pl.pallas_call(body, grid=(len(chosen), steps), in_specs=[blocks(width),...]
    ppermute x2, starting transfers between devices: 3.48 us -> 2.16 us  [the longest x1 1.62 us: computation(): lax.ppermute(below[:2], 'sp', shifted(sp_size, 4, 4, 1))]
  transfers between devices with their start and end apart: 12 -> 12, of which waited for: 4 -> 5; matrix products, arithmetic and copies ran while one was open for 2% -> 2% of each run, Pallas kernels for 22% -> 20%
where the time goes in v2:
time: 124 us; the launch traced here: 123 us
  Pallas kernels  30.7 us (25%)
  waiting for transfers between devices  25.8 us (21%)
  starting transfers between devices  24.5 us (20%)
  blocking collectives  24.2 us (20%)
  between operations  13.6 us (11%)
  local copies, waits for them, and re-layouts  3.15 us (3%)
    all_to_all x1, blocking collectives, computation(): attended = lax.all_to_all(attended, 'tp', 0, 0, tiled=True)  13.4 us
    ppermute x1, waiting for transfers between devices, computation(): below = lax.ppermute(ctx_line, 'sp', shifted(sp_size, 4, 4, 1))  11.2 us
    all_to_all x1, blocking collectives, copy_for_each(): lax.all_to_all(jnp.broadcast_to(shard[None], (length, *shard.shape)), axi...  10.8 us
    pallas_call x3, Pallas kernels, project(): pl.pallas_call(body, grid=(len(chosen), steps), in_specs=[blocks(width),...  8.47 us
    all_to_all x1, starting transfers between devices, computation(): summed = jnp.sum(lax.all_to_all(parts, 'sp', 0, 0, tiled=True), axis=0)  7.91 us
    pallas_call x1, Pallas kernels, attend_far(): pl.pallas_call(body, grid=(samples, rows_dev // per), in_specs=[rows_spec...  7.71 us
    pallas_call x1, Pallas kernels, finish(): pl.pallas_call(body, grid=(width // block,), in_specs=[whole(attended.sha...  5.79 us
    pallas_call x1, Pallas kernels, attend_near(): pl.pallas_call(body, grid=(samples, rows_dev // per), in_specs=[pl.BlockS...  5.76 us
  transfers between devices with their start and end apart: 12, of which 5 were waited for; matrix products, arithmetic and copies ran while one was open for 2% of the time, Pallas kernels for 20%

profile of v2, /device:TPU:32, one launch (start us, length us, event | category | flops | bytes accessed | tf_op | source)
XLA Modules:
  0.0 123.0 jit_solution(11440219317655231920)
XLA Ops:
  6.5 0.0 all-gather.3.cloned.1.call-start
  6.6 0.7 all-gather.3.cloned.1.call-update
  7.3 0.0 all-gather.5.cloned.1.call-start
  7.3 1.9 %modulation_parts.1 = f32[16,8,256]{2,1,0:T(8,128)} custom-call(s32[1]{0:T(128)} %bitcast.place_ref, bf16[2,2048]{1,0:T(2,128)(2,1)} %cond_ref.1, bf16[2048]{0:T(1024)(128)(2,1)} %ctx_ref.1, bf16[128,256]{1,0:T(8,128)(2,1)} %shift_ref.1, bf16[128,256]{1,0:T(8,128)(2,1)} %scale_ref.1, bf16[128,256]{1,0:T(8,128)(2,1)} %gate_ref.1), custom_call_target="tpu_custom_call" | custom-call | tf_op jit(solution)/shard_map/modulation_parts/pallas_call | solution.py:53
  9.3 0.0 all-gather.5.cloned.1.call-update
  9.3 7.9 %all-to-all-start = ((f32[16,8,256]{2,1,0:T(8,128)}), f32[16,8,256]{2,1,0:T(8,128)S(1)}, u32[]{:S(2)}, u32[]{:S(2)}) async-start(f32[16,8,256]{2,1,0:T(8,128)} %modulation_parts.1), calls=%async_computation | async-start | bytes 262144 | tf_op jit(solution)/shard_map/all_to_all | solution.py:445
  17.2 0.8 copy.20
  18.0 1.0 bias_table.1.table_ref
  19.0 0.0 copy-start.2
  19.0 1.2 %copy-done.2 = f32[2,256,896]{2,1,0:T(8,128)} copy-done((f32[2,256,896]{2,1,0:T(8,128)}, f32[2,256,896]{2,1,0:T(8,128)S(1)}, u32[]{:S(2)}) %copy-start.2) | copy-done | bytes 1835032
  20.2 3.3 %all-to-all-done = f32[16,8,256]{2,1,0:T(8,128)S(1)} async-done(((f32[16,8,256]{2,1,0:T(8,128)}), f32[16,8,256]{2,1,0:T(8,128)S(1)}, u32[]{:S(2)}, u32[]{:S(2)}) %all-to-all-start) | async-done | bytes 131104 | tf_op jit(solution)/shard_map/all_to_all | solution.py:445
  23.5 10.8 %all_to_all.15.tiles_ref.tile_ref = f32[8,8,256]{2,1,0:T(8,128)S(1)} all-to-all(f32[8,8,256]{2,1,0:T(8,128)S(1)} %broadcast_in_dim.14), channel_id=1, replica_groups=mesh['sp'=16,'tp'=8] {'tp'}, dimensions={0} | all-to-all | bytes 131072 | tf_op jit(solution)/shard_map/all_to_all | solution.py:22
  34.3 0.0 copy-done.6
  34.3 0.0 copy-done
  34.3 0.0 copy-done.1
  34.3 0.0 copy-start.5
  34.4 1.1 copy-done.5
  35.4 0.6 project.3
  36.1 0.6 collective-permute-start
  36.7 2.2 %collective-permute-start.1 = (bf16[2,64,512]{2,1,0:T(8,128)(2,1)S(1)}, bf16[2,64,512]{2,1,0:T(8,128)(2,1)}, u32[]{:S(2)}, u32[]{:S(2)}) collective-permute-start(bf16[2,64,512]{2,1,0:T(8,128)(2,1)S(1)} %bitcast.13), channel_id=1, source_target_pairs={{0,16},{8,24},{16,0},{24,8},{32,48},{40,56},{48,32},{56,40},{64,80... | collective-permute-start | bytes 393224 | tf_op jit(solution)/shard_map/ppermute | solution.py:415
  38.8 1.4 %collective-permute-start.2 = (bf16[2,64,512]{2,1,0:T(8,128)(2,1)S(1)}, bf16[2,64,512]{2,1,0:T(8,128)(2,1)}, u32[]{:S(2)}, u32[]{:S(2)}) collective-permute-start(bf16[2,64,512]{2,1,0:T(8,128)(2,1)S(1)} %bitcast.14), channel_id=1, source_target_pairs={{0,24},{8,0},{16,8},{24,16},{32,56},{40,32},{48,40},{56,48},{64,88... | collective-permute-start | bytes 393224 | tf_op jit(solution)/shard_map/ppermute | solution.py:415
  40.2 3.6 %all-gather.3.cloned.1.call-done.rows_ref = bf16[2,512,2048]{2,1,0:T(8,128)(2,1)} async-done(((bf16[2,64,2048]{2,1,0:T(8,128)(2,1)}), bf16[2,512,2048]{2,1,0:T(8,128)(2,1)}) %all-gather.3.cloned.1.call-update) | async-done | bytes 4194320 | tf_op jit(solution)/shard_map/all_gather | solution.py:440
  43.9 0.0 copy-done.4
  43.9 3.9 %project.4 = (bf16[2,512,512]{2,1,0:T(8,128)(2,1)S(1)}, bf16[2,512,256]{2,1,0:T(8,128)(2,1)S(1)}, bf16[2,192,512]{2,1,0:T(8,128)(2,1)S(1)}, bf16[2,256,512]{2,1,0:T(8,128)(2,1)S(1)}) custom-call(bf16[2,512,2048]{2,1,0:T(8,128)(2,1)} %all-gather.3.cloned.1.call-done.rows_ref, f32[1,2048]{1,0:T(1,128)S(1)} %bitcast.18, ...), custom_call_target="tpu_custom_call" | custom-call | tf_op jit(solution)/shard_map/project/pallas_call | solution.py:141
  47.8 0.0 collective-permute-done
  47.8 0.0 collective-permute-done.1
  47.8 0.0 collective-permute-done.2
  47.8 1.0 pad_maximum_fusion.refs_0_
  48.9 0.0 copy-start.7
  48.9 1.6 %collective-permute-start.5 = (bf16[4,2,64,512]{3,2,1,0:T(8,128)(2,1)S(1)}, bf16[4,2,64,512]{3,2,1,0:T(8,128)(2,1)S(1)}, u32[]{:S(2)}, u32[]{:S(2)}) collective-permute-start(bf16[4,2,64,512]{3,2,1,0:T(8,128)(2,1)S(1)} %pad_maximum_fusion.refs_0_), channel_id=1, source_target_pairs={{0,32},{8,40},{16,48},{24,56},{32,64},{40,72},{48,80},{56,88},{64,... | collective-permute-start | bytes 1572872 | tf_op jit(solution)/shard_map/ppermute | solution.py:472
  50.5 0.5 collective-permute-start.6
  51.0 3.9 %project.5 = (bf16[2,512,512]{2,1,0:T(8,128)(2,1)S(1)}, bf16[2,512,256]{2,1,0:T(8,128)(2,1)S(1)}, bf16[2,192,512]{2,1,0:T(8,128)(2,1)S(1)}, bf16[2,256,512]{2,1,0:T(8,128)(2,1)S(1)}) custom-call(bf16[2,512,2048]{2,1,0:T(8,128)(2,1)} %all-gather.3.cloned.1.call-done.rows_ref, ...), custom_call_target="tpu_custom_call", output_to_operand_aliasing={{0}: (6, {}), {1}: (7, {}), {2}: (8, {}), {3}: (9, {})} | custom-call | tf_op jit(solution)/shard_map/project/pallas_call | solution.py:141
  54.9 0.0 copy-start.3
  54.9 3.5 %collective-permute-start.3 = (bf16[2,256,512]{2,1,0:T(8,128)(2,1)S(1)}, bf16[2,256,512]{2,1,0:T(8,128)(2,1)S(1)}, u32[]{:S(2)}, u32[]{:S(2)}) collective-permute-start(bf16[2,256,512]{2,1,0:T(8,128)(2,1)S(1)} %get-tuple-element.39), channel_id=1, source_target_pairs={{0,8},{8,16},{16,24},{24,32},{32,40},{40,48},{48,56},{56,64},{64,7... | collective-permute-start | bytes 1572872 | tf_op jit(solution)/shard_map/ppermute | solution.py:485
  58.4 4.6 %collective-permute-start.4 = (bf16[2,192,512]{2,1,0:T(8,128)(2,1)S(1)}, bf16[2,192,512]{2,1,0:T(8,128)(2,1)S(1)}, u32[]{:S(2)}, u32[]{:S(2)}) collective-permute-start(bf16[2,192,512]{2,1,0:T(8,128)(2,1)S(1)} %get-tuple-element.41), channel_id=1, source_target_pairs={{8,0},{16,8},{24,16},{32,24},{40,32},{48,40},{56,48},{64,56},{72,6... | collective-permute-start | bytes 1179656 | tf_op jit(solution)/shard_map/ppermute | solution.py:486
  63.0 11.2 %collective-permute-done.5.refs_1_ = bf16[4,2,64,512]{3,2,1,0:T(8,128)(2,1)S(1)} collective-permute-done((bf16[4,2,64,512]{3,2,1,0:T(8,128)(2,1)S(1)}, bf16[4,2,64,512]{3,2,1,0:T(8,128)(2,1)S(1)}, u32[]{:S(2)}, u32[]{:S(2)}) %collective-permute-start.5) | collective-permute-done | bytes 524320 | tf_op jit(solution)/shard_map/ppermute | solution.py:472
  74.3 1.6 %collective-permute-start.7 = (bf16[2,2,64,512]{3,2,1,0:T(8,128)(2,1)S(1)}, bf16[2,2,64,512]{3,2,1,0:T(8,128)(2,1)S(1)}, u32[]{:S(2)}, u32[]{:S(2)}) collective-permute-start(bf16[2,2,64,512]{3,2,1,0:T(8,128)(2,1)S(1)} %slice.8), channel_id=1, source_target_pairs={{0,32},{8,40},{16,48},{24,56},{32,64},{40,72},{48,80},{56,88},{64,... | collective-permute-start | bytes 786440 | tf_op jit(solution)/shard_map/ppermute | solution.py:482
  75.9 0.0 collective-permute-done.6.refs_2_
  75.9 0.5 collective-permute-start.8
  76.5 5.6 %collective-permute-done.7.refs_3_ = bf16[2,2,64,512]{3,2,1,0:T(8,128)(2,1)S(1)} collective-permute-done((bf16[2,2,64,512]{3,2,1,0:T(8,128)(2,1)S(1)}, bf16[2,2,64,512]{3,2,1,0:T(8,128)(2,1)S(1)}, u32[]{:S(2)}, u32[]{:S(2)}) %collective-permute-start.7) | collective-permute-done | bytes 262176 | tf_op jit(solution)/shard_map/ppermute | solution.py:482
  82.0 1.4 %collective-permute-done.8.refs_4_ = bf16[2,2,64,512]{3,2,1,0:T(8,128)(2,1)S(1)} collective-permute-done((bf16[2,2,64,512]{3,2,1,0:T(8,128)(2,1)S(1)}, bf16[2,2,64,512]{3,2,1,0:T(8,128)(2,1)S(1)}, u32[]{:S(2)}, u32[]{:S(2)}) %collective-permute-start.8) | collective-permute-done | bytes 262176 | tf_op jit(solution)/shard_map/ppermute | solution.py:483
  83.4 0.0 copy-done.7
  83.4 7.7 %attend_far.1 = (f32[2,512,256]{2,1,0:T(8,128)S(1)}, f32[2,512,256]{2,1,0:T(8,128)S(1)}, f32[2,512,256]{2,1,0:T(8,128)S(1)}) custom-call(bf16[2,512,256]{2,1,0:T(8,128)(2,1)S(1)} %get-tuple-element.38.q_ref, bf16[4,2,64,512]{3,2,1,0:T(8,128)(2,1)S(1)} %pad_maximum_fusion.refs_0_, bf16[4,2,64,512]{3,2,1,0:T(8,128)(2,1)S(1)} %collective-permute-done.5.refs_1_, ...), custom_call_target="tpu_custom_call" | custom-call | tf_op jit(solution)/shard_map/attend_far/pallas_call | solution.py:356
  91.1 0.0 collective-permute-done.4.after_ref
  91.1 0.0 collective-permute-done.3.before_ref
  91.2 5.8 %attend_near.1 = bf16[8,2,64,256]{3,2,1,0:T(8,128)(2,1)S(1)} custom-call(s32[1]{0:T(128)} %bitcast.place_ref, bf16[2,512,256]{2,1,0:T(8,128)(2,1)S(1)} %get-tuple-element.38.q_ref, bf16[2,256,512]{2,1,0:T(8,128)(2,1)S(1)} %collective-permute-done.3.before_ref, bf16[2,512,512]{2,1,0:T(8,128)(2,1)S(1)} %get-tuple-element.40.pair_ref, ...), custom_call_target="tpu_custom_call" | custom-call | tf_op jit(solution)/shard_map/attend_near/pallas_call | solution.py:287
  96.9 13.4 %all_to_all.16.att_ref = bf16[8,128,256]{2,1,0:T(8,128)(2,1)} all-to-all(bf16[8,128,256]{2,1,0:T(8,128)(2,1)S(1)} %bitcast.10), channel_id=1, replica_groups=mesh['sp'=16,'tp'=8] {'tp'}, dimensions={0} | all-to-all | bytes 1048576 | tf_op jit(solution)/shard_map/all_to_all | solution.py:491
  110.4 5.8 %finish.1 = bf16[2,64,2048]{2,1,0:T(8,128)(2,1)} custom-call(bf16[8,128,256]{2,1,0:T(8,128)(2,1)} %all_to_all.16.att_ref, bf16[2048,2048]{1,0:T(8,128)(2,1)} %all-gather.5.cloned.1.call-done.w_ref, bf16[2,64,2048]{2,1,0:T(8,128)(2,1)} %latent_ref.1, f32[8,8,256]{2,1,0:T(8,128)S(1)} %all_to_all.15.tiles_ref.tile_ref), custom_call_target="tpu_custom_call" | custom-call | tf_op jit(solution)/shard_map/finish/pallas_call | solution.py:392
  (11 shorter events, 0.1 us)
Async XLA Ops:
  6.5 27.8 %copy-start.6 = (f32[2048]{0:T(1024)S(1)}, f32[2048]{0:T(1024)}, u32[]{:S(2)}) copy-start(f32[2048]{0:T(1024)} %param.21) | copy-start | bytes 24580
  6.5 27.8 %copy-start = (bf16[2048,256]{1,0:T(8,128)(2,1)S(1)}, bf16[2048,256]{1,0:T(8,128)(2,1)}, u32[]{:S(2)}) copy-start(bf16[2048,256]{1,0:T(8,128)(2,1)} %refs_0_.5) | copy-start | bytes 3145732
  6.5 27.8 %copy-start.1 = (bf16[2048,256]{1,0:T(8,128)(2,1)S(1)}, bf16[2048,256]{1,0:T(8,128)(2,1)}, u32[]{:S(2)}) copy-start(bf16[2048,256]{1,0:T(8,128)(2,1)} %refs_1_.5) | copy-start | bytes 3145732
  6.5 37.3 %copy-start.4 = (bf16[2048,256]{1,0:T(8,128)(2,1)S(1)}, bf16[2048,256]{1,0:T(8,128)(2,1)}, u32[]{:S(2)}) copy-start(bf16[2048,256]{1,0:T(8,128)(2,1)} %refs_2_.3) | copy-start | bytes 3145732
  6.5 37.3 %all-gather.3.cloned.1.call-start = ((), (), s32[]{:S(2)}) async-start(), calls=%async_computation.3 | async-start | bytes 4718592 | tf_op jit(solution)/shard_map/all_gather | solution.py:440
  7.3 103.1 %all-gather.5.cloned.1.call-start = ((), (), s32[]{:S(2)}) async-start(), calls=%async_computation.4 | async-start | bytes 9437184 | tf_op jit(solution)/shard_map/all_gather | solution.py:443
  9.3 14.2 %all-to-all-start = ((f32[16,8,256]{2,1,0:T(8,128)}), f32[16,8,256]{2,1,0:T(8,128)S(1)}, u32[]{:S(2)}, u32[]{:S(2)}) async-start(f32[16,8,256]{2,1,0:T(8,128)} %modulation_parts.1), calls=%async_computation | async-start | bytes 262144 | tf_op jit(solution)/shard_map/all_to_all | solution.py:445
  19.0 1.2 %copy-start.2 = (f32[2,256,896]{2,1,0:T(8,128)}, f32[2,256,896]{2,1,0:T(8,128)S(1)}, u32[]{:S(2)}) copy-start(f32[2,256,896]{2,1,0:T(8,128)S(1)} %bias_table.1.table_ref) | copy-start | bytes 5505028
  34.3 1.1 copy-start.5
  36.1 11.7 %collective-permute-start = (bf16[2,64,512]{2,1,0:T(8,128)(2,1)S(1)}, bf16[2,64,512]{2,1,0:T(8,128)(2,1)S(1)}, u32[]{:S(2)}, u32[]{:S(2)}) collective-permute-start(bf16[2,64,512]{2,1,0:T(8,128)(2,1)S(1)} %bitcast.12), channel_id=1, source_target_pairs={{0,8},{8,16},{16,24},{24,0},{32,40},{40,48},{48,56},{56,32},{64,72... | collective-permute-start | bytes 393224 | tf_op jit(solution)/shard_map/ppermute | solution.py:415
  36.7 11.2 %collective-permute-start.1 = (bf16[2,64,512]{2,1,0:T(8,128)(2,1)S(1)}, bf16[2,64,512]{2,1,0:T(8,128)(2,1)}, u32[]{:S(2)}, u32[]{:S(2)}) collective-permute-start(bf16[2,64,512]{2,1,0:T(8,128)(2,1)S(1)} %bitcast.13), channel_id=1, source_target_pairs={{0,16},{8,24},{16,0},{24,8},{32,48},{40,56},{48,32},{56,40},{64,80... | collective-permute-start | bytes 393224 | tf_op jit(solution)/shard_map/ppermute | solution.py:415
  38.8 9.0 %collective-permute-start.2 = (bf16[2,64,512]{2,1,0:T(8,128)(2,1)S(1)}, bf16[2,64,512]{2,1,0:T(8,128)(2,1)}, u32[]{:S(2)}, u32[]{:S(2)}) collective-permute-start(bf16[2,64,512]{2,1,0:T(8,128)(2,1)S(1)} %bitcast.14), channel_id=1, source_target_pairs={{0,24},{8,0},{16,8},{24,16},{32,56},{40,32},{48,40},{56,48},{64,88... | collective-permute-start | bytes 393224 | tf_op jit(solution)/shard_map/ppermute | solution.py:415
  48.9 34.5 %copy-start.7 = (f32[4]{0:T(128)S(1)}, f32[4]{0:T(128)}, u32[]{:S(2)}) copy-start(f32[4]{0:T(128)} %refs_5_.1) | copy-start | bytes 52
  48.9 25.4 %collective-permute-start.5 = (bf16[4,2,64,512]{3,2,1,0:T(8,128)(2,1)S(1)}, bf16[4,2,64,512]{3,2,1,0:T(8,128)(2,1)S(1)}, u32[]{:S(2)}, u32[]{:S(2)}) collective-permute-start(bf16[4,2,64,512]{3,2,1,0:T(8,128)(2,1)S(1)} %pad_maximum_fusion.refs_0_), channel_id=1, source_target_pairs={{0,32},{8,40},{16,48},{24,56},{32,64},{40,72},{48,80},{56,88},{64,... | collective-permute-start | bytes 1572872 | tf_op jit(solution)/shard_map/ppermute | solution.py:472
  50.5 25.4 %collective-permute-start.6 = (bf16[4,2,64,512]{3,2,1,0:T(8,128)(2,1)S(1)}, bf16[4,2,64,512]{3,2,1,0:T(8,128)(2,1)S(1)}, u32[]{:S(2)}, u32[]{:S(2)}) collective-permute-start(bf16[4,2,64,512]{3,2,1,0:T(8,128)(2,1)S(1)} %pad_maximum_fusion.refs_0_), channel_id=1, source_target_pairs={{0,96},{8,104},{16,112},{24,120},{32,0},{40,8},{48,16},{56,24},{64... | collective-permute-start | bytes 1572872 | tf_op jit(solution)/shard_map/ppermute | solution.py:473
  54.9 36.2 %copy-start.3 = (f32[2,256,896]{2,1,0:T(8,128)S(1)}, f32[2,256,896]{2,1,0:T(8,128)}, u32[]{:S(2)}) copy-start(f32[2,256,896]{2,1,0:T(8,128)} %copy-done.2) | copy-start | bytes 5505028
  54.9 36.2 %collective-permute-start.3 = (bf16[2,256,512]{2,1,0:T(8,128)(2,1)S(1)}, bf16[2,256,512]{2,1,0:T(8,128)(2,1)S(1)}, u32[]{:S(2)}, u32[]{:S(2)}) collective-permute-start(bf16[2,256,512]{2,1,0:T(8,128)(2,1)S(1)} %get-tuple-element.39), channel_id=1, source_target_pairs={{0,8},{8,16},{16,24},{24,32},{32,40},{40,48},{48,56},{56,64},{64,7... | collective-permute-start | bytes 1572872 | tf_op jit(solution)/shard_map/ppermute | solution.py:485
  58.4 32.7 %collective-permute-start.4 = (bf16[2,192,512]{2,1,0:T(8,128)(2,1)S(1)}, bf16[2,192,512]{2,1,0:T(8,128)(2,1)S(1)}, u32[]{:S(2)}, u32[]{:S(2)}) collective-permute-start(bf16[2,192,512]{2,1,0:T(8,128)(2,1)S(1)} %get-tuple-element.41), channel_id=1, source_target_pairs={{8,0},{16,8},{24,16},{32,24},{40,32},{48,40},{56,48},{64,56},{72,6... | collective-permute-start | bytes 1179656 | tf_op jit(solution)/shard_map/ppermute | solution.py:486
  74.3 7.8 %collective-permute-start.7 = (bf16[2,2,64,512]{3,2,1,0:T(8,128)(2,1)S(1)}, bf16[2,2,64,512]{3,2,1,0:T(8,128)(2,1)S(1)}, u32[]{:S(2)}, u32[]{:S(2)}) collective-permute-start(bf16[2,2,64,512]{3,2,1,0:T(8,128)(2,1)S(1)} %slice.8), channel_id=1, source_target_pairs={{0,32},{8,40},{16,48},{24,56},{32,64},{40,72},{48,80},{56,88},{64,... | collective-permute-start | bytes 786440 | tf_op jit(solution)/shard_map/ppermute | solution.py:482
  75.9 7.5 %collective-permute-start.8 = (bf16[2,2,64,512]{3,2,1,0:T(8,128)(2,1)S(1)}, bf16[2,2,64,512]{3,2,1,0:T(8,128)(2,1)S(1)}, u32[]{:S(2)}, u32[]{:S(2)}) collective-permute-start(bf16[2,2,64,512]{3,2,1,0:T(8,128)(2,1)S(1)} %slice.9), channel_id=1, source_target_pairs={{0,96},{8,104},{16,112},{24,120},{32,0},{40,8},{48,16},{56,24},{64... | collective-permute-start | bytes 786440 | tf_op jit(solution)/shard_map/ppermute | solution.py:483
Sparse Core Ops, SparseCore 0:
  9.0 34.7 all-gather.2
  45.6 49.6 all-gather.4

commit v3 on v2

--- a/solution.py
+++ b/solution.py
@@ -379,12 +379,11 @@
     first = modulation.shape[1] - samples
 
     def body(att_ref, w_ref, latent_ref, tile_ref, out_ref):
-        low = pl.program_id(0) * tiles
         everything = jnp.concatenate([att_ref[group] for group in range(groups)], axis=1)
         update = jnp.dot(everything, w_ref[...], preferred_element_type=jnp.float32)
         for s in range(samples):
             gate = jnp.concatenate(
-                [tile_ref[low + t, first + s : first + s + 1, :] for t in range(tiles)], axis=1
+                [tile_ref[t, first + s : first + s + 1, :] for t in range(tiles)], axis=1
             )
             part = update[s * tokens : (s + 1) * tokens]
             out_ref[s] = (latent_ref[s].astype(jnp.float32) + gate * part).astype(jnp.bfloat16)
@@ -396,7 +395,7 @@
             whole(attended.shape),
             pl.BlockSpec((width, block), lambda i: (0, i)),
             pl.BlockSpec((samples, tokens, block), lambda i: (0, 0, i)),
-            RESIDENT,
+            pl.BlockSpec((tiles, *modulation.shape[1:]), lambda i: (i, 0, 0)),
         ],
         out_specs=pl.BlockSpec((samples, tokens, block), lambda i: (0, 0, i)),
         out_shape=jax.ShapeDtypeStruct(latent.shape, latent.dtype),
@@ -451,7 +450,9 @@
     gain = norm_gain[None, :]
     ctx_rows = context.shape[1]
     (ctx_pair,) = project(
-        context.reshape(1, samples * ctx_rows, width),
+        pltpu.with_memory_space_constraint(
+            context.reshape(1, samples * ctx_rows, width), pltpu.HBM
+        ),
         gain,
         modulation,
         (w_key, w_value),
@@ -485,7 +486,7 @@
     before = resident(lax.ppermute(last, "sp", up))
     after = resident(lax.ppermute(first, "sp", down))
     ctx_pairs = [resident(array) for array in ctx_pairs]
-    far = attend_far(query, ctx_pairs, ctx_bias, 4)
+    far = attend_far(query, ctx_pairs, ctx_bias, 8)
     attended = attend_near(place, query, before, pair, after, table, far, rows_all, 4)
     attended = attended.reshape(tp_size, samples * tokens_dev, local_cols)
     attended = lax.all_to_all(attended, "tp", 0, 0, tiled=True)

time: 124 us -> 124 us (level)
    unnamed x17 -> x15, local copies, waits for them, and re-layouts: 3.1 us -> 2 us
  transfers between devices with their start and end apart: 12 -> 12, of which waited for: 5 -> 5; matrix products, arithmetic and copies ran while one was open for 2% -> 2% of each run, Pallas kernels for 20% -> 21%
where the time goes in v3:
time: 124 us; the launch traced here: 122 us
  Pallas kernels  31.2 us (25%)
  waiting for transfers between devices  25.8 us (21%)
  starting transfers between devices  24.5 us (20%)
  blocking collectives  24.2 us (20%)
  between operations  13.6 us (11%)
  local copies, waits for them, and re-layouts  2.05 us (2%)
    all_to_all x1, blocking collectives, computation(): attended = lax.all_to_all(attended, 'tp', 0, 0, tiled=True)  13.4 us
    ppermute x1, waiting for transfers between devices, computation(): below = lax.ppermute(ctx_line, 'sp', shifted(sp_size, 4, 4, 1))  11.2 us
    all_to_all x1, blocking collectives, copy_for_each(): lax.all_to_all(jnp.broadcast_to(shard[None], (length, *shard.shape)), axi...  10.8 us
    pallas_call x3, Pallas kernels, project(): pl.pallas_call(body, grid=(len(chosen), steps), in_specs=[blocks(width),...  9.59 us
    all_to_all x1, starting transfers between devices, computation(): summed = jnp.sum(lax.all_to_all(parts, 'sp', 0, 0, tiled=True), axis=0)  7.91 us
    pallas_call x1, Pallas kernels, attend_far(): pl.pallas_call(body, grid=(samples, rows_dev // per), in_specs=[rows_spec...  7.14 us
    pallas_call x1, Pallas kernels, finish(): pl.pallas_call(body, grid=(width // block,), in_specs=[whole(attended.sha...  5.79 us
    pallas_call x1, Pallas kernels, attend_near(): pl.pallas_call(body, grid=(samples, rows_dev // per), in_specs=[pl.BlockS...  5.75 us
  transfers between devices with their start and end apart: 12, of which 5 were waited for; matrix products, arithmetic and copies ran while one was open for 2% of the time, Pallas kernels for 21%

profile of v3, /device:TPU:32, one launch (start us, length us, event | category | flops | bytes accessed | tf_op | source)
XLA Modules:
  0.0 122.4 jit_solution(8090589242866649787)
XLA Ops:
  6.5 0.0 copy-start.5
  6.5 0.0 all-gather.3.cloned.1.call-start
  6.6 0.7 all-gather.3.cloned.1.call-update
  7.3 0.0 all-gather.5.cloned.1.call-start
  7.3 1.9 %modulation_parts.1 = f32[16,8,256]{2,1,0:T(8,128)} custom-call(s32[1]{0:T(128)} %bitcast.place_ref, bf16[2,2048]{1,0:T(2,128)(2,1)} %cond_ref.1, bf16[2048]{0:T(1024)(128)(2,1)} %ctx_ref.1, bf16[128,256]{1,0:T(8,128)(2,1)} %shift_ref.1, bf16[128,256]{1,0:T(8,128)(2,1)} %scale_ref.1, bf16[128,256]{1,0:T(8,128)(2,1)} %gate_ref.1), custom_call_target="tpu_custom_call" | custom-call | tf_op jit(solution)/shard_map/modulation_parts/pallas_call | solution.py:53
  9.3 0.0 all-gather.5.cloned.1.call-update
  9.3 7.9 %all-to-all-start = ((f32[16,8,256]{2,1,0:T(8,128)}), f32[16,8,256]{2,1,0:T(8,128)S(1)}, u32[]{:S(2)}, u32[]{:S(2)}) async-start(f32[16,8,256]{2,1,0:T(8,128)} %modulation_parts.1), calls=%async_computation | async-start | bytes 262144 | tf_op jit(solution)/shard_map/all_to_all | solution.py:444
  17.2 0.8 copy.20
  18.0 1.0 bias_table.1.table_ref
  19.0 0.0 copy-start.2
  19.0 1.2 copy-done.2
  20.2 3.3 %all-to-all-done = f32[16,8,256]{2,1,0:T(8,128)S(1)} async-done(((f32[16,8,256]{2,1,0:T(8,128)}), f32[16,8,256]{2,1,0:T(8,128)S(1)}, u32[]{:S(2)}, u32[]{:S(2)}) %all-to-all-start) | async-done | bytes 131104 | tf_op jit(solution)/shard_map/all_to_all | solution.py:444
  23.5 10.8 %all_to_all.15.tiles_ref.tile_ref = f32[8,8,256]{2,1,0:T(8,128)S(1)} all-to-all(f32[8,8,256]{2,1,0:T(8,128)S(1)} %broadcast_in_dim.14), channel_id=1, replica_groups=mesh['sp'=16,'tp'=8] {'tp'}, dimensions={0} | all-to-all | bytes 131072 | tf_op jit(solution)/shard_map/all_to_all | solution.py:22
  34.3 0.0 copy-done.5
  34.3 0.0 copy-done
  34.3 0.0 copy-done.1
  34.3 1.7 %project.3 = bf16[1,128,512]{2,1,0:T(8,128)(2,1)S(1)} custom-call(bf16[1,128,2048]{2,1,0:T(8,128)(2,1)} %bitcast.19, f32[1,2048]{1,0:T(1,128)S(1)} %bitcast.16, f32[8,8,256]{2,1,0:T(8,128)S(1)} %all_to_all.15.tiles_ref.tile_ref, bf16[2048,256]{1,0:T(8,128)(2,1)S(1)} %copy-done, bf16[2048,256]{1,0:T(8,128)(2,1)S(1)} %copy-done.1), custom_call_target="tpu_custom_call" | custom-call | tf_op jit(solution)/shard_map/project/pallas_call | solution.py:141
  36.1 0.6 collective-permute-start
  36.7 2.2 %collective-permute-start.1 = (bf16[2,64,512]{2,1,0:T(8,128)(2,1)S(1)}, bf16[2,64,512]{2,1,0:T(8,128)(2,1)}, u32[]{:S(2)}, u32[]{:S(2)}) collective-permute-start(bf16[2,64,512]{2,1,0:T(8,128)(2,1)S(1)} %bitcast.12), channel_id=1, source_target_pairs={{0,16},{8,24},{16,0},{24,8},{32,48},{40,56},{48,32},{56,40},{64,80... | collective-permute-start | bytes 393224 | tf_op jit(solution)/shard_map/ppermute | solution.py:414
  38.8 1.4 %collective-permute-start.2 = (bf16[2,64,512]{2,1,0:T(8,128)(2,1)S(1)}, bf16[2,64,512]{2,1,0:T(8,128)(2,1)}, u32[]{:S(2)}, u32[]{:S(2)}) collective-permute-start(bf16[2,64,512]{2,1,0:T(8,128)(2,1)S(1)} %bitcast.13), channel_id=1, source_target_pairs={{0,24},{8,0},{16,8},{24,16},{32,56},{40,32},{48,40},{56,48},{64,88... | collective-permute-start | bytes 393224 | tf_op jit(solution)/shard_map/ppermute | solution.py:414
  40.3 3.6 %all-gather.3.cloned.1.call-done.rows_ref = bf16[2,512,2048]{2,1,0:T(8,128)(2,1)} async-done(((bf16[2,64,2048]{2,1,0:T(8,128)(2,1)}), bf16[2,512,2048]{2,1,0:T(8,128)(2,1)}) %all-gather.3.cloned.1.call-update) | async-done | bytes 4194320 | tf_op jit(solution)/shard_map/all_gather | solution.py:439
  43.9 0.0 copy-done.4
  43.9 3.9 %project.4 = (bf16[2,512,512]{2,1,0:T(8,128)(2,1)S(1)}, bf16[2,512,256]{2,1,0:T(8,128)(2,1)S(1)}, bf16[2,192,512]{2,1,0:T(8,128)(2,1)S(1)}, bf16[2,256,512]{2,1,0:T(8,128)(2,1)S(1)}) custom-call(bf16[2,512,2048]{2,1,0:T(8,128)(2,1)} %all-gather.3.cloned.1.call-done.rows_ref, f32[1,2048]{1,0:T(1,128)S(1)} %bitcast.17, ...), custom_call_target="tpu_custom_call" | custom-call | tf_op jit(solution)/shard_map/project/pallas_call | solution.py:141
  47.8 0.0 collective-permute-done
  47.8 0.0 collective-permute-done.1
  47.8 0.0 collective-permute-done.2
  47.8 1.0 pad_maximum_fusion.refs_0_
  48.9 0.0 copy-start.6
  48.9 1.6 %collective-permute-start.5 = (bf16[4,2,64,512]{3,2,1,0:T(8,128)(2,1)S(1)}, bf16[4,2,64,512]{3,2,1,0:T(8,128)(2,1)S(1)}, u32[]{:S(2)}, u32[]{:S(2)}) collective-permute-start(bf16[4,2,64,512]{3,2,1,0:T(8,128)(2,1)S(1)} %pad_maximum_fusion.refs_0_), channel_id=1, source_target_pairs={{0,32},{8,40},{16,48},{24,56},{32,64},{40,72},{48,80},{56,88},{64,... | collective-permute-start | bytes 1572872 | tf_op jit(solution)/shard_map/ppermute | solution.py:473
  50.5 0.5 collective-permute-start.6
  51.0 3.9 %project.5 = (bf16[2,512,512]{2,1,0:T(8,128)(2,1)S(1)}, bf16[2,512,256]{2,1,0:T(8,128)(2,1)S(1)}, bf16[2,192,512]{2,1,0:T(8,128)(2,1)S(1)}, bf16[2,256,512]{2,1,0:T(8,128)(2,1)S(1)}) custom-call(bf16[2,512,2048]{2,1,0:T(8,128)(2,1)} %all-gather.3.cloned.1.call-done.rows_ref, ...), custom_call_target="tpu_custom_call", output_to_operand_aliasing={{0}: (6, {}), {1}: (7, {}), {2}: (8, {}), {3}: (9, {})} | custom-call | tf_op jit(solution)/shard_map/project/pallas_call | solution.py:141
  54.9 0.0 copy-start.3
  54.9 3.5 %collective-permute-start.3 = (bf16[2,256,512]{2,1,0:T(8,128)(2,1)S(1)}, bf16[2,256,512]{2,1,0:T(8,128)(2,1)S(1)}, u32[]{:S(2)}, u32[]{:S(2)}) collective-permute-start(bf16[2,256,512]{2,1,0:T(8,128)(2,1)S(1)} %get-tuple-element.39), channel_id=1, source_target_pairs={{0,8},{8,16},{16,24},{24,32},{32,40},{40,48},{48,56},{56,64},{64,7... | collective-permute-start | bytes 1572872 | tf_op jit(solution)/shard_map/ppermute | solution.py:486
  58.4 4.6 %collective-permute-start.4 = (bf16[2,192,512]{2,1,0:T(8,128)(2,1)S(1)}, bf16[2,192,512]{2,1,0:T(8,128)(2,1)S(1)}, u32[]{:S(2)}, u32[]{:S(2)}) collective-permute-start(bf16[2,192,512]{2,1,0:T(8,128)(2,1)S(1)} %get-tuple-element.41), channel_id=1, source_target_pairs={{8,0},{16,8},{24,16},{32,24},{40,32},{48,40},{56,48},{64,56},{72,6... | collective-permute-start | bytes 1179656 | tf_op jit(solution)/shard_map/ppermute | solution.py:487
  63.0 11.2 %collective-permute-done.5.refs_1_ = bf16[4,2,64,512]{3,2,1,0:T(8,128)(2,1)S(1)} collective-permute-done((bf16[4,2,64,512]{3,2,1,0:T(8,128)(2,1)S(1)}, bf16[4,2,64,512]{3,2,1,0:T(8,128)(2,1)S(1)}, u32[]{:S(2)}, u32[]{:S(2)}) %collective-permute-start.5) | collective-permute-done | bytes 524320 | tf_op jit(solution)/shard_map/ppermute | solution.py:473
  74.3 1.6 %collective-permute-start.7 = (bf16[2,2,64,512]{3,2,1,0:T(8,128)(2,1)S(1)}, bf16[2,2,64,512]{3,2,1,0:T(8,128)(2,1)S(1)}, u32[]{:S(2)}, u32[]{:S(2)}) collective-permute-start(bf16[2,2,64,512]{3,2,1,0:T(8,128)(2,1)S(1)} %slice.8), channel_id=1, source_target_pairs={{0,32},{8,40},{16,48},{24,56},{32,64},{40,72},{48,80},{56,88},{64,... | collective-permute-start | bytes 786440 | tf_op jit(solution)/shard_map/ppermute | solution.py:483
  75.9 0.0 collective-permute-done.6.refs_2_
  75.9 0.5 collective-permute-start.8
  76.5 5.6 %collective-permute-done.7.refs_3_ = bf16[2,2,64,512]{3,2,1,0:T(8,128)(2,1)S(1)} collective-permute-done((bf16[2,2,64,512]{3,2,1,0:T(8,128)(2,1)S(1)}, bf16[2,2,64,512]{3,2,1,0:T(8,128)(2,1)S(1)}, u32[]{:S(2)}, u32[]{:S(2)}) %collective-permute-start.7) | collective-permute-done | bytes 262176 | tf_op jit(solution)/shard_map/ppermute | solution.py:483
  82.0 1.4 %collective-permute-done.8.refs_4_ = bf16[2,2,64,512]{3,2,1,0:T(8,128)(2,1)S(1)} collective-permute-done((bf16[2,2,64,512]{3,2,1,0:T(8,128)(2,1)S(1)}, bf16[2,2,64,512]{3,2,1,0:T(8,128)(2,1)S(1)}, u32[]{:S(2)}, u32[]{:S(2)}) %collective-permute-start.8) | collective-permute-done | bytes 262176 | tf_op jit(solution)/shard_map/ppermute | solution.py:484
  83.4 0.0 copy-done.6
  83.4 7.1 %attend_far.1 = (f32[2,512,256]{2,1,0:T(8,128)S(1)}, f32[2,512,256]{2,1,0:T(8,128)S(1)}, f32[2,512,256]{2,1,0:T(8,128)S(1)}) custom-call(bf16[2,512,256]{2,1,0:T(8,128)(2,1)S(1)} %get-tuple-element.38.q_ref, bf16[4,2,64,512]{3,2,1,0:T(8,128)(2,1)S(1)} %pad_maximum_fusion.refs_0_, bf16[4,2,64,512]{3,2,1,0:T(8,128)(2,1)S(1)} %collective-permute-done.5.refs_1_, ...), custom_call_target="tpu_custom_call" | custom-call | tf_op jit(solution)/shard_map/attend_far/pallas_call | solution.py:356
  90.6 0.0 collective-permute-done.4.after_ref
  90.6 0.0 collective-permute-done.3.before_ref
  90.6 0.0 copy-done.3
  90.6 5.8 %attend_near.1 = bf16[8,2,64,256]{3,2,1,0:T(8,128)(2,1)S(1)} custom-call(s32[1]{0:T(128)} %bitcast.place_ref, bf16[2,512,256]{2,1,0:T(8,128)(2,1)S(1)} %get-tuple-element.38.q_ref, bf16[2,256,512]{2,1,0:T(8,128)(2,1)S(1)} %collective-permute-done.3.before_ref, bf16[2,512,512]{2,1,0:T(8,128)(2,1)S(1)} %get-tuple-element.40.pair_ref, ...), custom_call_target="tpu_custom_call" | custom-call | tf_op jit(solution)/shard_map/attend_near/pallas_call | solution.py:287
  96.4 13.4 %all_to_all.16.att_ref = bf16[8,128,256]{2,1,0:T(8,128)(2,1)} all-to-all(bf16[8,128,256]{2,1,0:T(8,128)(2,1)S(1)} %bitcast.10), channel_id=1, replica_groups=mesh['sp'=16,'tp'=8] {'tp'}, dimensions={0} | all-to-all | bytes 1048576 | tf_op jit(solution)/shard_map/all_to_all | solution.py:492
  109.8 5.8 %finish.1 = bf16[2,64,2048]{2,1,0:T(8,128)(2,1)} custom-call(bf16[8,128,256]{2,1,0:T(8,128)(2,1)} %all_to_all.16.att_ref, bf16[2048,2048]{1,0:T(8,128)(2,1)} %all-gather.5.cloned.1.call-done.w_ref, bf16[2,64,2048]{2,1,0:T(8,128)(2,1)} %latent_ref.1, f32[8,8,256]{2,1,0:T(8,128)S(1)} %all_to_all.15.tiles_ref.tile_ref), custom_call_target="tpu_custom_call" | custom-call | tf_op jit(solution)/shard_map/finish/pallas_call | solution.py:391
  (9 shorter events, 0.1 us)
Async XLA Ops:
  6.5 27.8 %copy-start.5 = (f32[2048]{0:T(1024)S(1)}, f32[2048]{0:T(1024)}, u32[]{:S(2)}) copy-start(f32[2048]{0:T(1024)} %param.21) | copy-start | bytes 24580
  6.5 27.8 %copy-start = (bf16[2048,256]{1,0:T(8,128)(2,1)S(1)}, bf16[2048,256]{1,0:T(8,128)(2,1)}, u32[]{:S(2)}) copy-start(bf16[2048,256]{1,0:T(8,128)(2,1)} %refs_0_.5) | copy-start | bytes 3145732
  6.5 27.8 %copy-start.1 = (bf16[2048,256]{1,0:T(8,128)(2,1)S(1)}, bf16[2048,256]{1,0:T(8,128)(2,1)}, u32[]{:S(2)}) copy-start(bf16[2048,256]{1,0:T(8,128)(2,1)} %refs_1_.5) | copy-start | bytes 3145732
  6.5 37.3 %copy-start.4 = (bf16[2048,256]{1,0:T(8,128)(2,1)S(1)}, bf16[2048,256]{1,0:T(8,128)(2,1)}, u32[]{:S(2)}) copy-start(bf16[2048,256]{1,0:T(8,128)(2,1)} %refs_2_.3) | copy-start | bytes 3145732
  6.5 37.3 %all-gather.3.cloned.1.call-start = ((), (), s32[]{:S(2)}) async-start(), calls=%async_computation.3 | async-start | bytes 4718592 | tf_op jit(solution)/shard_map/all_gather | solution.py:439
  7.3 102.5 %all-gather.5.cloned.1.call-start = ((), (), s32[]{:S(2)}) async-start(), calls=%async_computation.4 | async-start | bytes 9437184 | tf_op jit(solution)/shard_map/all_gather | solution.py:442
  9.3 14.2 %all-to-all-start = ((f32[16,8,256]{2,1,0:T(8,128)}), f32[16,8,256]{2,1,0:T(8,128)S(1)}, u32[]{:S(2)}, u32[]{:S(2)}) async-start(f32[16,8,256]{2,1,0:T(8,128)} %modulation_parts.1), calls=%async_computation | async-start | bytes 262144 | tf_op jit(solution)/shard_map/all_to_all | solution.py:444
  19.0 1.2 %copy-start.2 = (f32[2,256,896]{2,1,0:T(8,128)}, f32[2,256,896]{2,1,0:T(8,128)S(1)}, u32[]{:S(2)}) copy-start(f32[2,256,896]{2,1,0:T(8,128)S(1)} %bias_table.1.table_ref) | copy-start | bytes 5505028
  36.1 11.7 %collective-permute-start = (bf16[2,64,512]{2,1,0:T(8,128)(2,1)S(1)}, bf16[2,64,512]{2,1,0:T(8,128)(2,1)S(1)}, u32[]{:S(2)}, u32[]{:S(2)}) collective-permute-start(bf16[2,64,512]{2,1,0:T(8,128)(2,1)S(1)} %bitcast.11), channel_id=1, source_target_pairs={{0,8},{8,16},{16,24},{24,0},{32,40},{40,48},{48,56},{56,32},{64,72... | collective-permute-start | bytes 393224 | tf_op jit(solution)/shard_map/ppermute | solution.py:414
  36.7 11.1 %collective-permute-start.1 = (bf16[2,64,512]{2,1,0:T(8,128)(2,1)S(1)}, bf16[2,64,512]{2,1,0:T(8,128)(2,1)}, u32[]{:S(2)}, u32[]{:S(2)}) collective-permute-start(bf16[2,64,512]{2,1,0:T(8,128)(2,1)S(1)} %bitcast.12), channel_id=1, source_target_pairs={{0,16},{8,24},{16,0},{24,8},{32,48},{40,56},{48,32},{56,40},{64,80... | collective-permute-start | bytes 393224 | tf_op jit(solution)/shard_map/ppermute | solution.py:414
  38.8 9.0 %collective-permute-start.2 = (bf16[2,64,512]{2,1,0:T(8,128)(2,1)S(1)}, bf16[2,64,512]{2,1,0:T(8,128)(2,1)}, u32[]{:S(2)}, u32[]{:S(2)}) collective-permute-start(bf16[2,64,512]{2,1,0:T(8,128)(2,1)S(1)} %bitcast.13), channel_id=1, source_target_pairs={{0,24},{8,0},{16,8},{24,16},{32,56},{40,32},{48,40},{56,48},{64,88... | collective-permute-start | bytes 393224 | tf_op jit(solution)/shard_map/ppermute | solution.py:414
  48.9 34.5 %copy-start.6 = (f32[4]{0:T(128)S(1)}, f32[4]{0:T(128)}, u32[]{:S(2)}) copy-start(f32[4]{0:T(128)} %refs_5_.1) | copy-start | bytes 52
  48.9 25.4 %collective-permute-start.5 = (bf16[4,2,64,512]{3,2,1,0:T(8,128)(2,1)S(1)}, bf16[4,2,64,512]{3,2,1,0:T(8,128)(2,1)S(1)}, u32[]{:S(2)}, u32[]{:S(2)}) collective-permute-start(bf16[4,2,64,512]{3,2,1,0:T(8,128)(2,1)S(1)} %pad_maximum_fusion.refs_0_), channel_id=1, source_target_pairs={{0,32},{8,40},{16,48},{24,56},{32,64},{40,72},{48,80},{56,88},{64,... | collective-permute-start | bytes 1572872 | tf_op jit(solution)/shard_map/ppermute | solution.py:473
  50.5 25.4 %collective-permute-start.6 = (bf16[4,2,64,512]{3,2,1,0:T(8,128)(2,1)S(1)}, bf16[4,2,64,512]{3,2,1,0:T(8,128)(2,1)S(1)}, u32[]{:S(2)}, u32[]{:S(2)}) collective-permute-start(bf16[4,2,64,512]{3,2,1,0:T(8,128)(2,1)S(1)} %pad_maximum_fusion.refs_0_), channel_id=1, source_target_pairs={{0,96},{8,104},{16,112},{24,120},{32,0},{40,8},{48,16},{56,24},{64... | collective-permute-start | bytes 1572872 | tf_op jit(solution)/shard_map/ppermute | solution.py:474
  54.9 35.7 %copy-start.3 = (f32[2,256,896]{2,1,0:T(8,128)S(1)}, f32[2,256,896]{2,1,0:T(8,128)}, u32[]{:S(2)}) copy-start(f32[2,256,896]{2,1,0:T(8,128)} %copy-done.2) | copy-start | bytes 5505028
  54.9 35.7 %collective-permute-start.3 = (bf16[2,256,512]{2,1,0:T(8,128)(2,1)S(1)}, bf16[2,256,512]{2,1,0:T(8,128)(2,1)S(1)}, u32[]{:S(2)}, u32[]{:S(2)}) collective-permute-start(bf16[2,256,512]{2,1,0:T(8,128)(2,1)S(1)} %get-tuple-element.39), channel_id=1, source_target_pairs={{0,8},{8,16},{16,24},{24,32},{32,40},{40,48},{48,56},{56,64},{64,7... | collective-permute-start | bytes 1572872 | tf_op jit(solution)/shard_map/ppermute | solution.py:486
  58.4 32.1 %collective-permute-start.4 = (bf16[2,192,512]{2,1,0:T(8,128)(2,1)S(1)}, bf16[2,192,512]{2,1,0:T(8,128)(2,1)S(1)}, u32[]{:S(2)}, u32[]{:S(2)}) collective-permute-start(bf16[2,192,512]{2,1,0:T(8,128)(2,1)S(1)} %get-tuple-element.41), channel_id=1, source_target_pairs={{8,0},{16,8},{24,16},{32,24},{40,32},{48,40},{56,48},{64,56},{72,6... | collective-permute-start | bytes 1179656 | tf_op jit(solution)/shard_map/ppermute | solution.py:487
  74.3 7.8 %collective-permute-start.7 = (bf16[2,2,64,512]{3,2,1,0:T(8,128)(2,1)S(1)}, bf16[2,2,64,512]{3,2,1,0:T(8,128)(2,1)S(1)}, u32[]{:S(2)}, u32[]{:S(2)}) collective-permute-start(bf16[2,2,64,512]{3,2,1,0:T(8,128)(2,1)S(1)} %slice.8), channel_id=1, source_target_pairs={{0,32},{8,40},{16,48},{24,56},{32,64},{40,72},{48,80},{56,88},{64,... | collective-permute-start | bytes 786440 | tf_op jit(solution)/shard_map/ppermute | solution.py:483
  75.9 7.5 %collective-permute-start.8 = (bf16[2,2,64,512]{3,2,1,0:T(8,128)(2,1)S(1)}, bf16[2,2,64,512]{3,2,1,0:T(8,128)(2,1)S(1)}, u32[]{:S(2)}, u32[]{:S(2)}) collective-permute-start(bf16[2,2,64,512]{3,2,1,0:T(8,128)(2,1)S(1)} %slice.9), channel_id=1, source_target_pairs={{0,96},{8,104},{16,112},{24,120},{32,0},{40,8},{48,16},{56,24},{64... | collective-permute-start | bytes 786440 | tf_op jit(solution)/shard_map/ppermute | solution.py:484
Sparse Core Ops, SparseCore 0:
  9.0 34.7 all-gather.2
  45.6 49.6 all-gather.4

commit v4 on v3

--- a/solution.py
+++ b/solution.py
@@ -468,8 +468,7 @@
     ends = ((WIN_ROWS - REACH - 1) * GRID_W, REACH * GRID_W)
     w_triple = (w_key, w_value, w_query)
     outs = project(gathered, gain, modulation, w_triple, 0, 256, ends, 0)
-    ctx_pairs, outs = lax.optimization_barrier((ctx_pairs, outs))
-    ctx_line = jnp.stack(ctx_pairs)
+    ctx_line = stacked(ctx_pairs)
     below = lax.ppermute(ctx_line, "sp", shifted(sp_size, 4, 4, 1))
     above = lax.ppermute(ctx_line, "sp", shifted(sp_size, 4, 4, 3))
     for s in range(1, samples):
@@ -491,6 +490,21 @@
     attended = attended.reshape(tp_size, samples * tokens_dev, local_cols)
     attended = lax.all_to_all(attended, "tp", 0, 0, tiled=True)
     return finish(attended, w_out_all, latent, modulation, 4)
+
+
+def stacked(blocks):
+    def body(*refs):
+        for number in range(len(blocks)):
+            refs[-1][number] = refs[number][...]
+
+    return pl.pallas_call(
+        body,
+        in_specs=[RESIDENT] * len(blocks),
+        out_specs=RESIDENT,
+        out_shape=jax.ShapeDtypeStruct((len(blocks), *blocks[0].shape), blocks[0].dtype),
+        compiler_params=pltpu.CompilerParams(vmem_limit_bytes=8 * 2**20),
+        name="stacked",
+    )(*[resident(block) for block in blocks])
 
 
 def solution(mesh):

time: 124 us -> 122 us (0.984)
  waiting for transfers between devices: 25.8 us -> 20.3 us
  local copies, waits for them, and re-layouts: 2.05 us -> 3.96 us
  Pallas kernels: 31.2 us -> 32.9 us
    ppermute x1, waiting for transfers between devices: 11.2 us -> 0.01 us  [computation(): below = lax.ppermute(ctx_line, 'sp', shifted(sp_size, 4, 4, 1))]
    ppermute x3, waiting for transfers between devices: 0.01 us -> 5.46 us  [from_line(): lax.ppermute(block, axis, shifted(size, side, stride, value))]
    ppermute x1, waiting for transfers between devices: 5.58 us -> 10.8 us  [computation(): lax.ppermute(below[:2], 'sp', shifted(sp_size, 4, 4, 1))]
    all_gather x1, waiting for transfers between devices: 3.6 us -> 0.01 us  [computation(): gathered = lax.all_gather(latent, 'tp', axis=1, tiled=True)]
    ppermute x1, starting transfers between devices: 4.58 us -> 6.24 us  [computation(): after = resident(lax.ppermute(first, 'sp', down))]
    ppermute x1, starting transfers between devices: 1.62 us -> 0.07 us  [computation(): lax.ppermute(below[:2], 'sp', shifted(sp_size, 4, 4, 1))]
    ppermute x1, starting transfers between devices: 0.54 us -> 2.07 us  [computation(): lax.ppermute(above[2:], 'sp', shifted(sp_size, 4, 4, 3))]
    ppermute x1, waiting for transfers between devices: 1.37 us -> 0.01 us  [computation(): lax.ppermute(above[2:], 'sp', shifted(sp_size, 4, 4, 3))]
  transfers between devices with their start and end apart: 12 -> 12, of which waited for: 5 -> 4; matrix products, arithmetic and copies ran while one was open for 2% -> 2% of each run, Pallas kernels for 21% -> 22%
where the time goes in v4:
time: 122 us; the launch traced here: 120 us
  Pallas kernels  32.9 us (27%)
  starting transfers between devices  25.5 us (21%)
  blocking collectives  24.2 us (20%)
  waiting for transfers between devices  20.3 us (17%)
  between operations  13.6 us (11%)
  local copies, waits for them, and re-layouts  3.96 us (3%)
    all_to_all x1, blocking collectives, computation(): attended = lax.all_to_all(attended, 'tp', 0, 0, tiled=True)  13.4 us
    all_to_all x1, blocking collectives, copy_for_each(): lax.all_to_all(jnp.broadcast_to(shard[None], (length, *shard.shape)), axi...  10.8 us
    ppermute x1, waiting for transfers between devices, computation(): lax.ppermute(below[:2], 'sp', shifted(sp_size, 4, 4, 1))  10.8 us
    pallas_call x3, Pallas kernels, project(): pl.pallas_call(body, grid=(len(chosen), steps), in_specs=[blocks(width),...  9.61 us
    pallas_call x1, Pallas kernels, attend_far(): pl.pallas_call(body, grid=(samples, rows_dev // per), in_specs=[rows_spec...  7.95 us
    all_to_all x1, starting transfers between devices, computation(): summed = jnp.sum(lax.all_to_all(parts, 'sp', 0, 0, tiled=True), axis=0)  7.91 us
    ppermute x1, starting transfers between devices, computation(): after = resident(lax.ppermute(first, 'sp', down))  6.24 us
    pallas_call x1, Pallas kernels, finish(): pl.pallas_call(body, grid=(width // block,), in_specs=[whole(attended.sha...  5.79 us
  transfers between devices with their start and end apart: 12, of which 4 were waited for; matrix products, arithmetic and copies ran while one was open for 2% of the time, Pallas kernels for 22%

profile of v4, /device:TPU:32, one launch (start us, length us, event | category | flops | bytes accessed | tf_op | source)
XLA Modules:
  0.0 120.4 jit_solution(11042992959820636039)
XLA Ops:
  6.5 0.0 all-gather.3.cloned.1.call-start
  6.6 0.7 all-gather.3.cloned.1.call-update
  7.3 0.0 all-gather.5.cloned.1.call-start
  7.3 1.9 %modulation_parts.1 = f32[16,8,256]{2,1,0:T(8,128)} custom-call(s32[1]{0:T(128)} %bitcast.place_ref, bf16[2,2048]{1,0:T(2,128)(2,1)} %cond_ref.1, bf16[2048]{0:T(1024)(128)(2,1)} %ctx_ref.1, bf16[128,256]{1,0:T(8,128)(2,1)} %shift_ref.1, bf16[128,256]{1,0:T(8,128)(2,1)} %scale_ref.1, bf16[128,256]{1,0:T(8,128)(2,1)} %gate_ref.1), custom_call_target="tpu_custom_call" | custom-call | tf_op jit(solution)/shard_map/modulation_parts/pallas_call | solution.py:53
  9.3 0.0 all-gather.5.cloned.1.call-update
  9.3 7.9 %all-to-all-start = ((f32[16,8,256]{2,1,0:T(8,128)}), f32[16,8,256]{2,1,0:T(8,128)S(1)}, u32[]{:S(2)}, u32[]{:S(2)}) async-start(f32[16,8,256]{2,1,0:T(8,128)} %modulation_parts.1), calls=%async_computation | async-start | bytes 262144 | tf_op jit(solution)/shard_map/all_to_all | solution.py:444
  17.2 0.8 copy.20
  18.0 1.0 bias_table.1.table_ref
  19.0 0.0 copy-start.2
  19.0 1.2 %copy-done.2 = f32[2,256,896]{2,1,0:T(8,128)} copy-done((f32[2,256,896]{2,1,0:T(8,128)}, f32[2,256,896]{2,1,0:T(8,128)S(1)}, u32[]{:S(2)}) %copy-start.2) | copy-done | bytes 1835032
  20.2 3.3 %all-to-all-done = f32[16,8,256]{2,1,0:T(8,128)S(1)} async-done(((f32[16,8,256]{2,1,0:T(8,128)}), f32[16,8,256]{2,1,0:T(8,128)S(1)}, u32[]{:S(2)}, u32[]{:S(2)}) %all-to-all-start) | async-done | bytes 131104 | tf_op jit(solution)/shard_map/all_to_all | solution.py:444
  23.5 10.8 %all_to_all.15.tiles_ref.tile_ref = f32[8,8,256]{2,1,0:T(8,128)S(1)} all-to-all(f32[8,8,256]{2,1,0:T(8,128)S(1)} %broadcast_in_dim.14), channel_id=1, replica_groups=mesh['sp'=16,'tp'=8] {'tp'}, dimensions={0} | all-to-all | bytes 131072 | tf_op jit(solution)/shard_map/all_to_all | solution.py:22
  34.3 0.0 copy-done.5
  34.3 0.0 copy-done
  34.3 0.0 copy-done.1
  34.3 1.7 %project.5 = bf16[1,128,512]{2,1,0:T(8,128)(2,1)S(1)} custom-call(bf16[1,128,2048]{2,1,0:T(8,128)(2,1)} %bitcast.15, f32[1,2048]{1,0:T(1,128)S(1)} %bitcast.12, f32[8,8,256]{2,1,0:T(8,128)S(1)} %all_to_all.15.tiles_ref.tile_ref, bf16[2048,256]{1,0:T(8,128)(2,1)S(1)} %copy-done, bf16[2048,256]{1,0:T(8,128)(2,1)S(1)} %copy-done.1), custom_call_target="tpu_custom_call" | custom-call | tf_op jit(solution)/shard_map/project/pallas_call | solution.py:141
  36.1 0.6 collective-permute-start.2
  36.7 2.2 %collective-permute-start.3 = (bf16[2,64,512]{2,1,0:T(8,128)(2,1)S(1)}, bf16[2,64,512]{2,1,0:T(8,128)(2,1)S(1)}, u32[]{:S(2)}, u32[]{:S(2)}) collective-permute-start(bf16[2,64,512]{2,1,0:T(8,128)(2,1)S(1)} %bitcast.8), channel_id=1, source_target_pairs={{0,16},{8,24},{16,0},{24,8},{32,48},{40,56},{48,32},{56,40},{64,80... | collective-permute-start | bytes 393224 | tf_op jit(solution)/shard_map/ppermute | solution.py:414
  38.8 1.4 %collective-permute-start.4 = (bf16[2,64,512]{2,1,0:T(8,128)(2,1)S(1)}, bf16[2,64,512]{2,1,0:T(8,128)(2,1)S(1)}, u32[]{:S(2)}, u32[]{:S(2)}) collective-permute-start(bf16[2,64,512]{2,1,0:T(8,128)(2,1)S(1)} %bitcast.9), channel_id=1, source_target_pairs={{0,24},{8,0},{16,8},{24,16},{32,56},{40,32},{48,40},{56,48},{64,88... | collective-permute-start | bytes 393224 | tf_op jit(solution)/shard_map/ppermute | solution.py:414
  40.3 4.9 %collective-permute-done.2.refs_1_ = bf16[2,64,512]{2,1,0:T(8,128)(2,1)S(1)} collective-permute-done((bf16[2,64,512]{2,1,0:T(8,128)(2,1)S(1)}, bf16[2,64,512]{2,1,0:T(8,128)(2,1)S(1)}, u32[]{:S(2)}, u32[]{:S(2)}) %collective-permute-start.2) | collective-permute-done | bytes 131104 | tf_op jit(solution)/shard_map/ppermute | solution.py:414
  45.1 0.0 collective-permute-done.3.refs_2_
  45.1 0.6 collective-permute-done.4.refs_3_
  45.7 0.8 stacked.1.refs_0_
  46.5 0.6 collective-permute-start.5
  47.2 1.4 %collective-permute-start.6 = (bf16[4,2,64,512]{3,2,1,0:T(8,128)(2,1)}, bf16[4,2,64,512]{3,2,1,0:T(8,128)(2,1)}, u32[]{:S(2)}, u32[]{:S(2)}) collective-permute-start(bf16[4,2,64,512]{3,2,1,0:T(8,128)(2,1)} %stacked.1.refs_0_), channel_id=1, source_target_pairs={{0,96},{8,104},{16,112},{24,120},{32,0},{40,8},{48,16},{56,24},{64... | collective-permute-start | bytes 1572872 | tf_op jit(solution)/shard_map/ppermute | solution.py:473
  48.6 0.0 copy-done.4
  48.6 3.9 %project.3 = (bf16[2,512,512]{2,1,0:T(8,128)(2,1)S(1)}, bf16[2,512,256]{2,1,0:T(8,128)(2,1)S(1)}, bf16[2,192,512]{2,1,0:T(8,128)(2,1)S(1)}, bf16[2,256,512]{2,1,0:T(8,128)(2,1)S(1)}) custom-call(bf16[2,512,2048]{2,1,0:T(8,128)(2,1)} %all-gather.3.cloned.1.call-done.rows_ref, f32[1,2048]{1,0:T(1,128)S(1)} %bitcast.13, ...), custom_call_target="tpu_custom_call" | custom-call | tf_op jit(solution)/shard_map/project/pallas_call | solution.py:141
  52.5 0.0 copy-start.6
  52.5 3.9 %project.4 = (bf16[2,512,512]{2,1,0:T(8,128)(2,1)S(1)}, bf16[2,512,256]{2,1,0:T(8,128)(2,1)S(1)}, bf16[2,192,512]{2,1,0:T(8,128)(2,1)S(1)}, bf16[2,256,512]{2,1,0:T(8,128)(2,1)S(1)}) custom-call(bf16[2,512,2048]{2,1,0:T(8,128)(2,1)} %all-gather.3.cloned.1.call-done.rows_ref, ...), custom_call_target="tpu_custom_call", output_to_operand_aliasing={{0}: (6, {}), {1}: (7, {}), {2}: (8, {}), {3}: (9, {})} | custom-call | tf_op jit(solution)/shard_map/project/pallas_call | solution.py:141
  56.5 0.0 copy-start.3
  56.5 2.9 %collective-permute-start = (bf16[2,256,512]{2,1,0:T(8,128)(2,1)S(1)}, bf16[2,256,512]{2,1,0:T(8,128)(2,1)S(1)}, u32[]{:S(2)}, u32[]{:S(2)}) collective-permute-start(bf16[2,256,512]{2,1,0:T(8,128)(2,1)S(1)} %get-tuple-element.27), channel_id=1, source_target_pairs={{0,8},{8,16},{16,24},{24,32},{32,40},{40,48},{48,56},{56,64},{64,7... | collective-permute-start | bytes 1572872 | tf_op jit(solution)/shard_map/ppermute | solution.py:485
  59.4 6.2 %collective-permute-start.1 = (bf16[2,192,512]{2,1,0:T(8,128)(2,1)S(1)}, bf16[2,192,512]{2,1,0:T(8,128)(2,1)S(1)}, u32[]{:S(2)}, u32[]{:S(2)}) collective-permute-start(bf16[2,192,512]{2,1,0:T(8,128)(2,1)S(1)} %get-tuple-element.29), channel_id=1, source_target_pairs={{8,0},{16,8},{24,16},{32,24},{40,32},{48,40},{56,48},{64,56},{72,6... | collective-permute-start | bytes 1179656 | tf_op jit(solution)/shard_map/ppermute | solution.py:486
  65.7 0.0 collective-permute-done.5.refs_1_
  65.7 1.0 slice.8
  66.7 0.1 collective-permute-start.7
  66.8 0.0 collective-permute-done.6.refs_2_
  66.8 1.0 slice.9
  67.7 2.1 %collective-permute-start.8 = (bf16[2,2,64,512]{3,2,1,0:T(8,128)(2,1)S(1)}, bf16[2,2,64,512]{3,2,1,0:T(8,128)(2,1)S(1)}, u32[]{:S(2)}, u32[]{:S(2)}) collective-permute-start(bf16[2,2,64,512]{3,2,1,0:T(8,128)(2,1)S(1)} %slice.9), channel_id=1, source_target_pairs={{0,96},{8,104},{16,112},{24,120},{32,0},{40,8},{48,16},{56,24},{64... | collective-permute-start | bytes 786440 | tf_op jit(solution)/shard_map/ppermute | solution.py:483
  69.8 10.8 %collective-permute-done.7.refs_3_ = bf16[2,2,64,512]{3,2,1,0:T(8,128)(2,1)S(1)} collective-permute-done((bf16[2,2,64,512]{3,2,1,0:T(8,128)(2,1)S(1)}, bf16[2,2,64,512]{3,2,1,0:T(8,128)(2,1)S(1)}, u32[]{:S(2)}, u32[]{:S(2)}) %collective-permute-start.7) | collective-permute-done | bytes 262176 | tf_op jit(solution)/shard_map/ppermute | solution.py:482
  80.6 0.0 collective-permute-done.8.refs_4_
  80.6 0.0 copy-done.6
  80.6 7.9 %attend_far.1 = (f32[2,512,256]{2,1,0:T(8,128)S(1)}, f32[2,512,256]{2,1,0:T(8,128)S(1)}, f32[2,512,256]{2,1,0:T(8,128)S(1)}) custom-call(bf16[2,512,256]{2,1,0:T(8,128)(2,1)S(1)} %get-tuple-element.26.q_ref, bf16[4,2,64,512]{3,2,1,0:T(8,128)(2,1)} %stacked.1.refs_0_, bf16[4,2,64,512]{3,2,1,0:T(8,128)(2,1)} %collective-permute-done.5.refs_1_, ...), custom_call_target="tpu_custom_call" | custom-call | tf_op jit(solution)/shard_map/attend_far/pallas_call | solution.py:356
  88.6 0.0 collective-permute-done.1.after_ref
  88.6 0.0 collective-permute-done.before_ref
  88.6 0.0 copy-done.3
  88.6 5.8 %attend_near.1 = bf16[8,2,64,256]{3,2,1,0:T(8,128)(2,1)S(1)} custom-call(s32[1]{0:T(128)} %bitcast.place_ref, bf16[2,512,256]{2,1,0:T(8,128)(2,1)S(1)} %get-tuple-element.26.q_ref, bf16[2,256,512]{2,1,0:T(8,128)(2,1)S(1)} %collective-permute-done.before_ref, bf16[2,512,512]{2,1,0:T(8,128)(2,1)S(1)} %get-tuple-element.28.pair_ref, ...), custom_call_target="tpu_custom_call" | custom-call | tf_op jit(solution)/shard_map/attend_near/pallas_call | solution.py:287
  94.3 13.4 %all_to_all.16.att_ref = bf16[8,128,256]{2,1,0:T(8,128)(2,1)} all-to-all(bf16[8,128,256]{2,1,0:T(8,128)(2,1)S(1)} %bitcast.6), channel_id=1, replica_groups=mesh['sp'=16,'tp'=8] {'tp'}, dimensions={0} | all-to-all | bytes 1048576 | tf_op jit(solution)/shard_map/all_to_all | solution.py:491
  107.8 5.8 %finish.1 = bf16[2,64,2048]{2,1,0:T(8,128)(2,1)} custom-call(bf16[8,128,256]{2,1,0:T(8,128)(2,1)} %all_to_all.16.att_ref, bf16[2048,2048]{1,0:T(8,128)(2,1)} %all-gather.5.cloned.1.call-done.w_ref, bf16[2,64,2048]{2,1,0:T(8,128)(2,1)} %latent_ref.1, f32[8,8,256]{2,1,0:T(8,128)S(1)} %all_to_all.15.tiles_ref.tile_ref), custom_call_target="tpu_custom_call" | custom-call | tf_op jit(solution)/shard_map/finish/pallas_call | solution.py:391
  (9 shorter events, 0.0 us)
Async XLA Ops:
  6.5 27.8 %copy-start.5 = (f32[2048]{0:T(1024)S(1)}, f32[2048]{0:T(1024)}, u32[]{:S(2)}) copy-start(f32[2048]{0:T(1024)} %param.21) | copy-start | bytes 24580
  6.5 27.8 %copy-start = (bf16[2048,256]{1,0:T(8,128)(2,1)S(1)}, bf16[2048,256]{1,0:T(8,128)(2,1)}, u32[]{:S(2)}) copy-start(bf16[2048,256]{1,0:T(8,128)(2,1)} %refs_0_.5) | copy-start | bytes 3145732
  6.5 27.8 %copy-start.1 = (bf16[2048,256]{1,0:T(8,128)(2,1)S(1)}, bf16[2048,256]{1,0:T(8,128)(2,1)}, u32[]{:S(2)}) copy-start(bf16[2048,256]{1,0:T(8,128)(2,1)} %refs_1_.5) | copy-start | bytes 3145732
  6.5 42.0 %copy-start.4 = (bf16[2048,256]{1,0:T(8,128)(2,1)S(1)}, bf16[2048,256]{1,0:T(8,128)(2,1)}, u32[]{:S(2)}) copy-start(bf16[2048,256]{1,0:T(8,128)(2,1)} %refs_2_.3) | copy-start | bytes 3145732
  6.5 42.0 %all-gather.3.cloned.1.call-start = ((), (), s32[]{:S(2)}) async-start(), calls=%async_computation.3 | async-start | bytes 4718592 | tf_op jit(solution)/shard_map/all_gather | solution.py:439
  7.3 100.5 %all-gather.5.cloned.1.call-start = ((), (), s32[]{:S(2)}) async-start(), calls=%async_computation.4 | async-start | bytes 9437184 | tf_op jit(solution)/shard_map/all_gather | solution.py:442
  9.3 14.2 %all-to-all-start = ((f32[16,8,256]{2,1,0:T(8,128)}), f32[16,8,256]{2,1,0:T(8,128)S(1)}, u32[]{:S(2)}, u32[]{:S(2)}) async-start(f32[16,8,256]{2,1,0:T(8,128)} %modulation_parts.1), calls=%async_computation | async-start | bytes 262144 | tf_op jit(solution)/shard_map/all_to_all | solution.py:444
  19.0 1.2 %copy-start.2 = (f32[2,256,896]{2,1,0:T(8,128)}, f32[2,256,896]{2,1,0:T(8,128)S(1)}, u32[]{:S(2)}) copy-start(f32[2,256,896]{2,1,0:T(8,128)S(1)} %bias_table.1.table_ref) | copy-start | bytes 5505028
  36.1 9.1 %collective-permute-start.2 = (bf16[2,64,512]{2,1,0:T(8,128)(2,1)S(1)}, bf16[2,64,512]{2,1,0:T(8,128)(2,1)S(1)}, u32[]{:S(2)}, u32[]{:S(2)}) collective-permute-start(bf16[2,64,512]{2,1,0:T(8,128)(2,1)S(1)} %bitcast.7), channel_id=1, source_target_pairs={{0,8},{8,16},{16,24},{24,0},{32,40},{40,48},{48,56},{56,32},{64,72... | collective-permute-start | bytes 393224 | tf_op jit(solution)/shard_map/ppermute | solution.py:414
  36.7 8.5 %collective-permute-start.3 = (bf16[2,64,512]{2,1,0:T(8,128)(2,1)S(1)}, bf16[2,64,512]{2,1,0:T(8,128)(2,1)S(1)}, u32[]{:S(2)}, u32[]{:S(2)}) collective-permute-start(bf16[2,64,512]{2,1,0:T(8,128)(2,1)S(1)} %bitcast.8), channel_id=1, source_target_pairs={{0,16},{8,24},{16,0},{24,8},{32,48},{40,56},{48,32},{56,40},{64,80... | collective-permute-start | bytes 393224 | tf_op jit(solution)/shard_map/ppermute | solution.py:414
  38.8 6.9 %collective-permute-start.4 = (bf16[2,64,512]{2,1,0:T(8,128)(2,1)S(1)}, bf16[2,64,512]{2,1,0:T(8,128)(2,1)S(1)}, u32[]{:S(2)}, u32[]{:S(2)}) collective-permute-start(bf16[2,64,512]{2,1,0:T(8,128)(2,1)S(1)} %bitcast.9), channel_id=1, source_target_pairs={{0,24},{8,0},{16,8},{24,16},{32,56},{40,32},{48,40},{56,48},{64,88... | collective-permute-start | bytes 393224 | tf_op jit(solution)/shard_map/ppermute | solution.py:414
  46.5 19.2 %collective-permute-start.5 = (bf16[4,2,64,512]{3,2,1,0:T(8,128)(2,1)}, bf16[4,2,64,512]{3,2,1,0:T(8,128)(2,1)}, u32[]{:S(2)}, u32[]{:S(2)}) collective-permute-start(bf16[4,2,64,512]{3,2,1,0:T(8,128)(2,1)} %stacked.1.refs_0_), channel_id=1, source_target_pairs={{0,32},{8,40},{16,48},{24,56},{32,64},{40,72},{48,80},{56,88},{64,... | collective-permute-start | bytes 1572872 | tf_op jit(solution)/shard_map/ppermute | solution.py:472
  47.2 19.6 %collective-permute-start.6 = (bf16[4,2,64,512]{3,2,1,0:T(8,128)(2,1)}, bf16[4,2,64,512]{3,2,1,0:T(8,128)(2,1)}, u32[]{:S(2)}, u32[]{:S(2)}) collective-permute-start(bf16[4,2,64,512]{3,2,1,0:T(8,128)(2,1)} %stacked.1.refs_0_), channel_id=1, source_target_pairs={{0,96},{8,104},{16,112},{24,120},{32,0},{40,8},{48,16},{56,24},{64... | collective-permute-start | bytes 1572872 | tf_op jit(solution)/shard_map/ppermute | solution.py:473
  52.5 28.1 %copy-start.6 = (f32[4]{0:T(128)S(1)}, f32[4]{0:T(128)}, u32[]{:S(2)}) copy-start(f32[4]{0:T(128)} %refs_5_.1) | copy-start | bytes 52
  56.5 32.1 %copy-start.3 = (f32[2,256,896]{2,1,0:T(8,128)S(1)}, f32[2,256,896]{2,1,0:T(8,128)}, u32[]{:S(2)}) copy-start(f32[2,256,896]{2,1,0:T(8,128)} %copy-done.2) | copy-start | bytes 5505028
  56.5 32.1 %collective-permute-start = (bf16[2,256,512]{2,1,0:T(8,128)(2,1)S(1)}, bf16[2,256,512]{2,1,0:T(8,128)(2,1)S(1)}, u32[]{:S(2)}, u32[]{:S(2)}) collective-permute-start(bf16[2,256,512]{2,1,0:T(8,128)(2,1)S(1)} %get-tuple-element.27), channel_id=1, source_target_pairs={{0,8},{8,16},{16,24},{24,32},{32,40},{40,48},{48,56},{56,64},{64,7... | collective-permute-start | bytes 1572872 | tf_op jit(solution)/shard_map/ppermute | solution.py:485
  59.4 29.1 %collective-permute-start.1 = (bf16[2,192,512]{2,1,0:T(8,128)(2,1)S(1)}, bf16[2,192,512]{2,1,0:T(8,128)(2,1)S(1)}, u32[]{:S(2)}, u32[]{:S(2)}) collective-permute-start(bf16[2,192,512]{2,1,0:T(8,128)(2,1)S(1)} %get-tuple-element.29), channel_id=1, source_target_pairs={{8,0},{16,8},{24,16},{32,24},{40,32},{48,40},{56,48},{64,56},{72,6... | collective-permute-start | bytes 1179656 | tf_op jit(solution)/shard_map/ppermute | solution.py:486
  66.7 13.9 %collective-permute-start.7 = (bf16[2,2,64,512]{3,2,1,0:T(8,128)(2,1)S(1)}, bf16[2,2,64,512]{3,2,1,0:T(8,128)(2,1)S(1)}, u32[]{:S(2)}, u32[]{:S(2)}) collective-permute-start(bf16[2,2,64,512]{3,2,1,0:T(8,128)(2,1)S(1)} %slice.8), channel_id=1, source_target_pairs={{0,32},{8,40},{16,48},{24,56},{32,64},{40,72},{48,80},{56,88},{64,... | collective-permute-start | bytes 786440 | tf_op jit(solution)/shard_map/ppermute | solution.py:482
  67.7 12.8 %collective-permute-start.8 = (bf16[2,2,64,512]{3,2,1,0:T(8,128)(2,1)S(1)}, bf16[2,2,64,512]{3,2,1,0:T(8,128)(2,1)S(1)}, u32[]{:S(2)}, u32[]{:S(2)}) collective-permute-start(bf16[2,2,64,512]{3,2,1,0:T(8,128)(2,1)S(1)} %slice.9), channel_id=1, source_target_pairs={{0,96},{8,104},{16,112},{24,120},{32,0},{40,8},{48,16},{56,24},{64... | collective-permute-start | bytes 786440 | tf_op jit(solution)/shard_map/ppermute | solution.py:483
Sparse Core Ops, SparseCore 0:
  9.0 34.7 all-gather.2
  45.6 49.5 all-gather.4
